TPU v7x, 256 devices: a whole 4x4x8 slice. The times are simulated.
256 devices in a mesh: gr: 2 (over z_hi), sp: 16 (over z_lo, y), tp: 8 (over x, core).
Axes of the slice: x: 4, y: 4, z: 8 (z_hi: 2, z_lo: 4; z = z_hi * 4 + z_lo), core: 2. Of those that a mesh axis runs over, the one named last changes fastest.
Arguments:
- prompt: bfloat16 [256, 256, 1024], P('gr', 'sp'), parts along dimension 0, may hold values from -6 to 6
- w_key: bfloat16 [1024, 8, 128], P(None, 'tp'), may hold values from -0.1875 to 0.1875
- w_value: bfloat16 [1024, 8, 128], P(None, 'tp'), may hold values from -0.1875 to 0.1875
- w_in_gate: bfloat16 [2, 1024, 8], P(None, None, 'tp'), may hold values from -0.1875 to 0.1875
- w_forget_gate: bfloat16 [2, 1024, 8], P(None, None, 'tp'), may hold values from -0.1875 to 0.1875
- in_bias: float32 [2, 8], P(None, 'tp'), may hold values from -6 to 0, as said below
- forget_bias: float32 [2, 8], P(None, 'tp'), may hold values from 1 to 10, as said below
- query: bfloat16 [256, 8, 128], P(('gr', 'sp'), 'tp'), parts along dimension 0, may hold values from -6 to 6
- w_out: bfloat16 [8, 128, 1024], P('tp'), may hold values from -0.5 to 0.5
Outputs:
- memory: bfloat16 [2, 256, 8, 128, 128], P(None, ('gr', 'sp'), 'tp'), parts along dimension 1
- normalizer: float32 [2, 256, 8, 128], P(None, ('gr', 'sp'), 'tp'), parts along dimension 1
- stabilizer: float32 [2, 256, 8], P(None, ('gr', 'sp'), 'tp'), parts along dimension 1
- read: bfloat16 [256, 1024], P(('gr', 'sp'), 'tp'), parts along dimension 0
There are 2 independent parts, one for each index of `gr`. A program takes and returns all parts, laid end to end along the dimension named above; an argument that names none is the same for every part. Nothing has to cross between parts.
Inputs may be any that keep to these rules, and one draw needn't show every extreme that they name: forget_bias lies between 1 and 10; the per-head share of memory kept over the whole prompt is spread between a few and some ninety percent. in_bias lies between -6 and 0.
All inputs are finite; a program needn't handle non-finite values.
Results may differ from a plain program's by a relative error of at most 0.015.
Values may be sent and summed in bfloat16 or wider, within the bound.
A program may use at most 64 MiB of HBM per device.

v0:
```python
import jax
import jax.numpy as jnp
from jax import lax
from jax.sharding import Mesh
from jax.sharding import PartitionSpec as P

TP = ("tp_0", "tp_1")


highest = lax.Precision.DEFAULT


def in_blocks(array, dim, size):
    shape = array.shape
    parts = array.reshape(*shape[:dim], size, shape[dim] // size, *shape[dim + 1 :])
    return jnp.moveaxis(parts, dim, 0)


def cut_rows(length, count):
    hop = length // count
    if hop >= 8:
        hop -= hop % 8
    return [hop * k for k in range(1, count)]


def sum_in_order(parts, axes, turns):
    inside = parts.shape[1:]
    parts = parts.reshape(*(lax.axis_size(a) for a in axes), *inside)
    parts = jnp.moveaxis(parts, turns, range(len(axes))).reshape(-1, *inside)
    for k in turns:
        parts = lax.psum_scatter(parts, axes[k], scatter_dimension=0, tiled=True)
    return parts[0]


def sum_all_axes(array, axes, dim):
    parts = in_blocks(array, dim, lax.axis_size(axes))
    cut = max(range(1, max(2, parts.ndim - 1)), key=lambda d: parts.shape[d])
    count, gathered = len(axes), []
    for initial, slab in enumerate(jnp.split(parts, cut_rows(parts.shape[cut], count), axis=cut)):
        if slab.size:
            turns = [(initial + k) % count for k in range(count)]
            gathered.append(sum_in_order(slab, axes, turns))
    return jnp.concatenate(gathered, axis=cut - 1)


def project(token_rows, w_key, w_value, w_in_gate, w_forget_gate, in_bias, forget_bias):
    key_rows = jnp.einsum(
        "bsd,dhe->bshe", token_rows, w_key, preferred_element_type=jnp.float32
    ).astype(jnp.bfloat16)
    value_rows = jnp.einsum(
        "bsd,dhe->bshe", token_rows, w_value, preferred_element_type=jnp.float32
    ).astype(jnp.bfloat16)
    in_pre = (
        jnp.einsum("bsd,gdh->bsgh", token_rows, w_in_gate, preferred_element_type=jnp.float32)
        + in_bias
    )
    forget_pre = (
        jnp.einsum("bsd,gdh->bsgh", token_rows, w_forget_gate, preferred_element_type=jnp.float32)
        + forget_bias
    )
    return (key_rows, value_rows, jnp.stack((in_pre, forget_pre), axis=2))


def summary(scaled, float_values, in_log, forget_log, backward):
    total_forget = jnp.sum(forget_log, axis=1)
    running = jnp.cumsum(forget_log, axis=1)
    if backward:
        log_weight = in_log + running - forget_log
    else:
        log_weight = in_log + total_forget[:, None, :] - running
    stable = jnp.maximum(total_forget, jnp.max(log_weight, axis=1))
    weight = jnp.exp(log_weight - stable[:, None, :])
    weighted = scaled * weight[..., None]
    memory = jnp.einsum("bshd,bshe->bhde", weighted, float_values, precision=highest)
    normal = jnp.sum(weighted, axis=1)
    return (memory, normal, stable)


def read_out(memory_bf, normal, stable, query_f):
    cells = memory_bf.astype(jnp.float32)
    numerator = jnp.sum(query_f[..., :, None] * cells, axis=-2)
    denominator = jnp.sum(query_f * normal, axis=-1)
    floor_value = jnp.maximum(jnp.maximum(jnp.abs(denominator), jnp.exp(-stable)), 1.0)
    return numerator / floor_value[..., None]


def shards(prompt, w_key, w_value, w_in_gate, w_forget_gate, in_bias, forget_bias, query, w_out):
    key_rows, value_rows, gate_values = project(
        prompt, w_key, w_value, w_in_gate, w_forget_gate, in_bias, forget_bias
    )
    key_rows, value_rows = (
        lax.all_to_all(key_rows, "sp", split_axis=0, concat_axis=1, tiled=True),
        lax.all_to_all(value_rows, "sp", split_axis=0, concat_axis=1, tiled=True),
    )
    gate_values = lax.all_to_all(gate_values, "sp", split_axis=0, concat_axis=1, tiled=True)
    scaled = key_rows.astype(jnp.float32) * key_rows.shape[-1] ** (-0.5)
    float_values = value_rows.astype(jnp.float32)
    query_f = query.astype(jnp.float32)
    memories = []
    normals = []
    stables = []
    reads = []
    for course in range(2):
        memory, normal, stable = summary(
            scaled,
            float_values,
            gate_values[:, :, 0, course, :],
            jax.nn.log_sigmoid(gate_values[:, :, 1, course, :]),
            course == 1,
        )
        memory_bf = memory.astype(jnp.bfloat16)
        memories.append(memory_bf)
        normals.append(normal)
        stables.append(stable)
        reads.append(read_out(memory_bf, normal, stable, query_f))
    hidden = (reads[0] + reads[1]).astype(jnp.bfloat16)
    head_terms = jnp.einsum("bhd,hde->be", hidden, w_out, preferred_element_type=jnp.float32)
    read = sum_all_axes(head_terms, TP, 1).astype(jnp.bfloat16)
    return (jnp.stack(memories), jnp.stack(normals), jnp.stack(stables), read)


def solution(mesh):
    torus = Mesh(
        mesh.devices.reshape(mesh.shape["gr"], mesh.shape["sp"], 4, 2), ("gr", "sp", "tp_0", "tp_1")
    )
    return jax.shard_map(
        shards,
        mesh=torus,
        in_specs=(
            P("gr", "sp", None),
            P(None, TP, None),
            P(None, TP, None),
            P(None, None, TP),
            P(None, None, TP),
            P(None, TP),
            P(None, TP),
            P(("gr", "sp"), TP, None),
            P(TP, None, None),
        ),
        out_specs=(
            P(None, ("gr", "sp"), TP, None, None),
            P(None, ("gr", "sp"), TP, None),
            P(None, ("gr", "sp"), TP),
            P(("gr", "sp"), TP),
        ),
        check_vma=False,
    )
```

profile of v0, /device:TPU:1, one launch (start us, length us, event | category | flops | bytes accessed | tf_op | source)
XLA Modules:
  0.0 103.9 jit_solution(10119917832557531772)
XLA Ops:
  0.6 0.0 copy-start
  0.6 0.0 copy-start.1
  0.7 7.3 %fusion.2 = f32[128,16,1,2,1]{1,3,0,4,2:T(2,128)S(1)} fusion(bf16[128,16,1024]{2,1,0:T(8,128)(2,1)} %param.9, bf16[2,1024,1]{1,0,2:T(2,128)(2,1)} %param.13, f32[2]{0:T(128)} %bitcast.310), kind=kOutput, calls=%fused_computation.7 | convolution fusion | flops 8392704 | bytes 4214792 | tf_op jit(solution)/shard_map/bsd,gdh->bsgh/dot_general | solution.py:58
  8.0 0.0 copy-done.7
  8.0 0.0 copy-start.3
  8.1 5.0 %fusion.3 = f32[128,16,1,2,1]{1,3,0,4,2:T(2,128)S(1)} fusion(bf16[128,16,1024]{2,1,0:T(8,128)(2,1)S(1)} %copy-done.1, bf16[2,1024,1]{1,0,2:T(2,128)(2,1)S(1)} %copy-done.6, f32[2]{0:T(128)S(1)} %bitcast.311), kind=kOutput, calls=%fused_computation.9 | convolution fusion | flops 8392704 | bytes 4214792 | tf_op jit(solution)/shard_map/bsd,gdh->bsgh/dot_general | solution.py:54
  13.0 0.1 copy_bitcast_fusion.1
  13.2 0.9 reshape.807
  14.1 9.2 %all-to-all-start.1 = ((f32[16,1,512]{2,1,0:T(1,128)}), f32[16,1,512]{2,1,0:T(1,128)S(1)}, u32[]{:S(2)}, u32[]{:S(2)}) async-start(f32[16,1,512]{2,1,0:T(1,128)} %reshape.807), calls=%async_computation.1 | async-start | bytes 65536 | tf_op jit(solution)/shard_map/all_to_all | solution.py:95
  23.3 0.0 copy-start.2
  23.3 0.0 copy-start.5
  23.3 0.0 copy-start.4
  23.4 0.0 copy-start.9
  23.4 0.0 copy-start.8
  23.4 4.4 %fusion = bf16[128,16,1,128]{3,1,2,0:T(8,128)(2,1)} fusion(bf16[128,16,1024]{2,1,0:T(8,128)(2,1)} %param.9, bf16[1024,1,128]{2,0,1:T(8,128)(2,1)S(1)} %copy-done), kind=kOutput, calls=%fused_computation.2 | convolution fusion | flops 537133056 | bytes 4980736 | tf_op jit(solution)/shard_map/bsd,dhe->bshe/dot_general | solution.py:47
  27.8 2.1 %fusion.1 = bf16[128,16,1,128]{3,1,2,0:T(8,128)(2,1)} fusion(bf16[128,16,1024]{2,1,0:T(8,128)(2,1)S(1)} %copy-done.2, bf16[1024,1,128]{2,0,1:T(8,128)(2,1)S(1)} %copy-done.3), kind=kOutput, calls=%fused_computation.3 | convolution fusion | flops 537133056 | bytes 4980736 | tf_op jit(solution)/shard_map/bsd,dhe->bshe/dot_general | solution.py:50
  29.8 0.2 copy.197
  30.0 0.6 dynamic-slice.2
  30.6 0.6 dynamic-slice
  32.5 0.0 all-to-all-done.1
  32.5 7.0 %all-to-all-start = ((bf16[128,16,1,128]{3,1,2,0:T(8,128)(2,1)}), bf16[128,16,1,128]{3,1,2,0:T(8,128)(2,1)S(1)}, u32[]{:S(2)}, u32[]{:S(2)}) async-start(bf16[128,16,1,128]{3,1,2,0:T(8,128)(2,1)} %fusion), calls=%async_computation | async-start | bytes 1048576 | tf_op jit(solution)/shard_map/all_to_all | solution.py:92
  39.5 0.5 broadcast.249
  40.0 0.7 reduce.18
  40.7 0.4 reshape.808
  41.2 0.1 all_to_all.35
  41.3 0.1 fusion.15
  41.5 0.6 reduce-window.16
  42.1 0.2 slice_reduce_fusion
  42.3 0.6 reduce-window.14
  42.9 0.2 slice_reduce_fusion.1
  43.1 0.1 copy.189
  43.2 0.1 copy.186
  43.3 0.2 fusion.44
  43.5 0.1 squeeze.29
  43.6 0.1 broadcast.236
  43.6 0.1 reshape.789
  43.7 0.1 reshape.788
  43.8 0.1 neg.209
  43.9 0.1 fusion.14
  44.1 0.1 broadcast.234
  44.1 0.1 reshape.787
  44.2 0.1 reshape.786
  44.3 0.1 squeeze.28
  44.4 0.1 exponential_multiply_fusion
  44.5 0.6 pad_maximum_fusion.3
  45.1 0.1 fusion.48
  45.2 7.3 %all-to-all-done = bf16[128,16,1,128]{3,1,2,0:T(8,128)(2,1)S(1)} async-done(((bf16[128,16,1,128]{3,1,2,0:T(8,128)(2,1)}), bf16[128,16,1,128]{3,1,2,0:T(8,128)(2,1)S(1)}, u32[]{:S(2)}, u32[]{:S(2)}) %all-to-all-start) | async-done | bytes 524320 | tf_op jit(solution)/shard_map/all_to_all | solution.py:92
  52.5 7.1 %all-to-all-start.2 = ((bf16[128,16,1,128]{3,1,2,0:T(8,128)(2,1)}), bf16[128,16,1,128]{3,1,2,0:T(8,128)(2,1)S(1)}, u32[]{:S(2)}, u32[]{:S(2)}) async-start(bf16[128,16,1,128]{3,1,2,0:T(8,128)(2,1)} %fusion.1), calls=%async_computation.2 | async-start | bytes 1048576 | tf_op jit(solution)/shard_map/all_to_all | solution.py:93
  59.7 0.1 convert_bitcast_fusion
  59.8 0.1 copy.164
  59.9 0.6 multiply_reduce_fusion.1
  60.5 0.1 fusion.54
  60.7 12.7 %all-to-all-done.2 = bf16[128,16,1,128]{3,1,2,0:T(8,128)(2,1)S(1)} async-done(((bf16[128,16,1,128]{3,1,2,0:T(8,128)(2,1)}), bf16[128,16,1,128]{3,1,2,0:T(8,128)(2,1)S(1)}, u32[]{:S(2)}, u32[]{:S(2)}) %all-to-all-start.2) | async-done | bytes 524320 | tf_op jit(solution)/shard_map/all_to_all | solution.py:93
  73.4 0.8 convolution_convert_fusion.2
  74.2 0.9 multiply_reduce_fusion.3
  75.1 0.2 convolution_bitcast_fusion
  75.3 5.9 %all-reduce.2 = f32[8,4,128]{2,1,0:T(4,128)S(1)} all-reduce(f32[8,4,128]{2,1,0:T(4,128)S(1)} %bitcast.302), channel_id=4, replica_groups=mesh['gr'=2,'sp'=16,'tp_0'=4,'tp_1'=2] {'tp_1'}, use_global_device_ids=true, to_apply=%region_16.17.clone | all-reduce | flops 4096 | bytes 32768
  81.3 13.3 %all-reduce.4 = (bf16[4,4,128]{2,1,0:T(4,128)(2,1)S(1)}, f32[8,4,128]{2,1,0:T(4,128)S(1)}) all-reduce(f32[4,4,128]{2,1,0:T(4,128)S(1)} %constant_dynamic-slice_fusion, f32[8,4,128]{2,1,0:T(4,128)S(1)} %get-tuple-element.39), channel_id=5, replica_groups=mesh['gr'=2,'sp'=16,'tp_0'=4,'tp_1'=2] {'tp_0'}, use_global_device_ids=true, to_apply=%region_17.18.clone | all-reduce | flops 6144 | bytes 45056
  94.5 6.1 %all-reduce.1 = bf16[2,4,128]{2,1,0:T(4,128)(2,1)S(1)} all-reduce(f32[2,4,128]{2,1,0:T(4,128)S(1)} %constant_dynamic-slice_fusion.1), channel_id=3, replica_groups=mesh['gr'=2,'sp'=16,'tp_0'=4,'tp_1'=2] {'tp_1'}, use_global_device_ids=true, to_apply=%region_15.16.clone | all-reduce | flops 1024 | bytes 6144
  100.6 0.6 fusion.61
  101.3 0.7 fusion.62
  101.9 0.6 pad_maximum_fusion.2
  102.5 0.6 pad_maximum_fusion.1
  103.1 0.8 maximum_bitcast_fusion
  (35 shorter events, 0.4 us)
Async XLA Ops:
  0.6 22.7 %copy-start = (bf16[1024,1,128]{2,0,1:T(8,128)(2,1)S(1)}, bf16[1024,1,128]{2,0,1:T(8,128)(2,1)}, u32[]{:S(2)}) copy-start(bf16[1024,1,128]{2,0,1:T(8,128)(2,1)} %param.10) | copy-start | bytes 786436
  0.6 7.4 %copy-start.1 = (bf16[128,16,1024]{2,1,0:T(8,128)(2,1)S(1)}, bf16[128,16,1024]{2,1,0:T(8,128)(2,1)}, u32[]{:S(2)}) copy-start(bf16[128,16,1024]{2,1,0:T(8,128)(2,1)} %param.9) | copy-start | bytes 12582916
  0.7 7.4 %copy-start.7 = (f32[2,1]{0,1:T(1,128)S(1)}, f32[2,1]{0,1:T(1,128)}, u32[]{:S(2)}) copy-start(f32[2,1]{0,1:T(1,128)} %param.14) | copy-start | bytes 28
  0.7 7.4 %copy-start.6 = (bf16[2,1024,1]{1,0,2:T(2,128)(2,1)S(1)}, bf16[2,1024,1]{1,0,2:T(2,128)(2,1)}, u32[]{:S(2)}) copy-start(bf16[2,1024,1]{1,0,2:T(2,128)(2,1)} %param.12) | copy-start | bytes 12292
  8.0 19.7 %copy-start.3 = (bf16[1024,1,128]{2,0,1:T(8,128)(2,1)S(1)}, bf16[1024,1,128]{2,0,1:T(8,128)(2,1)}, u32[]{:S(2)}) copy-start(bf16[1024,1,128]{2,0,1:T(8,128)(2,1)} %param.11) | copy-start | bytes 786436
  14.1 18.4 %all-to-all-start.1 = ((f32[16,1,512]{2,1,0:T(1,128)}), f32[16,1,512]{2,1,0:T(1,128)S(1)}, u32[]{:S(2)}, u32[]{:S(2)}) async-start(f32[16,1,512]{2,1,0:T(1,128)} %reshape.807), calls=%async_computation.1 | async-start | bytes 65536 | tf_op jit(solution)/shard_map/all_to_all | solution.py:95
  23.3 4.5 %copy-start.2 = (bf16[128,16,1024]{2,1,0:T(8,128)(2,1)S(1)}, bf16[128,16,1024]{2,1,0:T(8,128)(2,1)}, u32[]{:S(2)}) copy-start(bf16[128,16,1024]{2,1,0:T(8,128)(2,1)} %param.9) | copy-start | bytes 12582916
  23.3 6.5 %copy-start.5 = (bf16[8,1,128]{2,0,1:T(8,128)(2,1)S(1)}, bf16[8,1,128]{2,0,1:T(8,128)(2,1)}, u32[]{:S(2)}) copy-start(bf16[8,1,128]{2,0,1:T(8,128)(2,1)} %param.16) | copy-start | bytes 6148
  23.3 6.5 %copy-start.4 = (bf16[1,128,1024]{2,1,0:T(8,128)(2,1)S(1)}, bf16[1,128,1024]{2,1,0:T(8,128)(2,1)}, u32[]{:S(2)}) copy-start(bf16[1,128,1024]{2,1,0:T(8,128)(2,1)} %param.17) | copy-start | bytes 786436
  23.4 6.7 %copy-start.9 = (u32[256]{0:T(256)S(1)}, u32[256]{0:T(256)}, u32[]{:S(2)}) copy-start(u32[256]{0:T(256)} %constant.30) | copy-start | bytes 3076
  23.4 7.2 %copy-start.8 = (u32[256]{0:T(256)S(1)}, u32[256]{0:T(256)}, u32[]{:S(2)}) copy-start(u32[256]{0:T(256)} %constant.26) | copy-start | bytes 3076
  32.5 20.0 %all-to-all-start = ((bf16[128,16,1,128]{3,1,2,0:T(8,128)(2,1)}), bf16[128,16,1,128]{3,1,2,0:T(8,128)(2,1)S(1)}, u32[]{:S(2)}, u32[]{:S(2)}) async-start(bf16[128,16,1,128]{3,1,2,0:T(8,128)(2,1)} %fusion), calls=%async_computation | async-start | bytes 1048576 | tf_op jit(solution)/shard_map/all_to_all | solution.py:92
  52.5 20.8 %all-to-all-start.2 = ((bf16[128,16,1,128]{3,1,2,0:T(8,128)(2,1)}), bf16[128,16,1,128]{3,1,2,0:T(8,128)(2,1)S(1)}, u32[]{:S(2)}, u32[]{:S(2)}) async-start(bf16[128,16,1,128]{3,1,2,0:T(8,128)(2,1)} %fusion.1), calls=%async_computation.2 | async-start | bytes 1048576 | tf_op jit(solution)/shard_map/all_to_all | solution.py:93
where the time goes:
time: 104 us
  blocking collectives  25.3 us (24%)
  starting transfers between devices  23.3 us (22%)
  matrix products  20.6 us (20%)
  waiting for transfers between devices  20 us (19%)
  other arithmetic  6.27 us (6%)
  local copies, waits for them, and re-layouts  6.19 us (6%)
  between operations  2.33 us (2%)
    unnamed x3, blocking collectives  25.3 us
    all_to_all x1, waiting for transfers between devices, shards(): lax.all_to_all(value_rows, 'sp', split_axis=0, concat_axis=1, tiled=True)  12.7 us
    all_to_all x1, starting transfers between devices, shards(): lax.all_to_all(gate_values, 'sp', split_axis=0, concat_axis=1, tiled=True)  9.18 us
    dot_general x1, matrix products, project(): jnp.einsum('bsd,gdh->bsgh', token_rows, w_forget_gate, preferred_element_...  7.33 us
    all_to_all x1, waiting for transfers between devices, shards(): lax.all_to_all(key_rows, 'sp', split_axis=0, concat_axis=1, tiled=True)  7.32 us
    all_to_all x1, starting transfers between devices, shards(): lax.all_to_all(value_rows, 'sp', split_axis=0, concat_axis=1, tiled=True)  7.15 us
    all_to_all x1, starting transfers between devices, shards(): lax.all_to_all(key_rows, 'sp', split_axis=0, concat_axis=1, tiled=True)  6.95 us
    dot_general x1, matrix products, project(): jnp.einsum('bsd,gdh->bsgh', token_rows, w_in_gate, preferred_element_type...  4.97 us
  transfers between devices with their start and end apart: 3, of which 2 were waited for; matrix products, arithmetic and copies ran while one was open for 14% of the time, Pallas kernels for 0%

commit v1 on v0

v1 whole, which is shorter than its diff:
```python
import functools

import jax
import jax.numpy as jnp
from jax import lax
from jax.experimental import pallas as pl
from jax.experimental.pallas import tpu as pltpu
from jax.sharding import Mesh
from jax.sharding import PartitionSpec as P

MESH = pl.DeviceIdType.MESH
TP = ("x", "c")
F32 = jnp.float32
BF16 = jnp.bfloat16
FAR = 12


def offsets(k):
    return lax.rem(k, 3) + 1, k // 3


def kernel(
    prompt, w_key, w_value, w_gate, in_bias, forget_bias, query, w_out,
    memory_out, normal_out, stable_out, read_out,
    rows, weights, gate_w, out_w, keys, values, gates, terms, parts,
    load_sem, far_send, far_recv, near_send, near_recv, x_send, x_recv, swap_send, swap_recv, term_send, term_recv,
):
    z, y, x, c = (lax.axis_index(a) for a in ("z", "y", "x", "c"))
    here = z * 4 + y
    seq = 4 * c + x
    up = lax.rem(x + 1 + 2 * c, 4)
    down = lax.rem(x + 3 + 2 * c, 4)
    across = lax.rem(x + 2, 4)

    loads = [
        pltpu.make_async_copy(w_key, weights.at[:, pl.ds(0, 128)], load_sem.at[0]),
        pltpu.make_async_copy(w_value, weights.at[:, pl.ds(128, 128)], load_sem.at[1]),
        pltpu.make_async_copy(prompt.at[pl.ds(here * 8, 8)], rows.at[here], load_sem.at[2]),
        pltpu.make_async_copy(w_out, out_w, load_sem.at[3]),
    ]
    for load in loads:
        load.start()

    barrier = pltpu.get_barrier_semaphore()

    @pl.loop(1, 16)
    def _(k):
        to = {"z": lax.rem(z + k // 4, 4), "y": lax.rem(y + lax.rem(k, 4), 4)}
        pl.semaphore_signal(barrier, inc=1, device_id=to, device_id_type=MESH)

    @pl.loop(1, 8)
    def _(k):
        to = {"x": lax.rem(x + k // 2, 4), "c": lax.rem(c + lax.rem(k, 2), 2)}
        pl.semaphore_signal(barrier, inc=1, device_id=to, device_id_type=MESH)

    pl.semaphore_wait(barrier, 22)

    def far(k):
        dz, dy = offsets(k)
        tz, ty = lax.rem(z + dz, 4), lax.rem(y + dy, 4)
        return pltpu.make_async_remote_copy(
            src_ref=prompt.at[(tz * 4 + ty) * 8 + seq],
            dst_ref=rows.at[here, seq],
            send_sem=far_send.at[k],
            recv_sem=far_recv.at[k],
            device_id={"z": tz, "y": ty},
            device_id_type=MESH,
        )

    def near(k):
        ty = lax.rem(y + k + 1, 4)
        return pltpu.make_async_remote_copy(
            src_ref=prompt.at[pl.ds((z * 4 + ty) * 8 + 4 * c, 4)],
            dst_ref=rows.at[here, pl.ds(4 * c, 4)],
            send_sem=near_send.at[k],
            recv_sem=near_recv.at[k],
            device_id={"y": ty},
            device_id_type=MESH,
        )

    def source(k):
        dz, dy = offsets(k)
        return lax.rem(z + 4 - dz, 4) * 4 + lax.rem(y + 4 - dy, 4)

    def near_source(k):
        return z * 4 + lax.rem(y + 3 - k, 4)

    def along_x(k, which):
        held = seq if which < 2 else 4 * c + down
        block = rows.at[source(k), held]
        return pltpu.make_async_remote_copy(
            src_ref=block,
            dst_ref=block,
            send_sem=x_send.at[k, which],
            recv_sem=x_recv.at[k, which],
            device_id={"x": down if which == 1 else up},
            device_id_type=MESH,
        )

    def swap(k, src):
        block = rows.at[src, pl.ds(4 * c, 4)]
        return pltpu.make_async_remote_copy(
            src_ref=block,
            dst_ref=block,
            send_sem=swap_send.at[k],
            recv_sem=swap_recv.at[k],
            device_id={"c": 1 - c},
            device_id_type=MESH,
        )

    @pl.loop(0, FAR)
    def _(k):
        far(k).start()

    @pl.loop(0, 3)
    def _(k):
        near(k).start()

    lane8 = lax.broadcasted_iota(jnp.int32, (8, 128), 1) // 8
    gate8 = lax.broadcasted_iota(jnp.int32, (8, 128), 0)
    spread = jnp.where(lane8 == gate8, 1.0, 0.0).astype(BF16)
    gate_w[...] = lax.dot_general(
        w_gate[...], spread, (((0,), (0,)), ((), ())), preferred_element_type=F32
    ).astype(BF16)

    lane = lax.broadcasted_iota(jnp.int32, (8, 16, 128), 2)
    which_seq = lax.broadcasted_iota(jnp.int32, (8, 16, 128), 0)
    own_lane = lax.rem(lane, 8) == which_seq

    def project(src):
        block = rows[src].reshape(128, 1024)
        both = jnp.dot(block, weights[...], preferred_element_type=F32)
        at = pl.ds(pl.multiple_of(src * 16, 16), 16)
        keys[:, at, :] = both[:, :128].astype(BF16).reshape(8, 16, 128)
        values[:, at, :] = both[:, 128:].astype(BF16).reshape(8, 16, 128)
        pre = jnp.dot(block, gate_w[...], preferred_element_type=F32).reshape(8, 16, 128)
        gates[at, :] = jnp.sum(jnp.where(own_lane, pre, 0.0), axis=0)

    for load in loads:
        load.wait()
    project(here)

    @pl.loop(0, FAR + 3)
    def _(step):
        @pl.when(step < FAR)
        def _():
            far(step).wait_recv()
            along_x(step, 0).start()
            along_x(step, 1).start()

        @pl.when((step >= 1) & (step < FAR + 1))
        def _():
            along_x(step - 1, 0).wait_recv()
            along_x(step - 1, 2).start()

        @pl.when((step >= 2) & (step < FAR + 2))
        def _():
            along_x(step - 2, 1).wait_recv()
            along_x(step - 2, 2).wait_recv()
            swap(step - 2, source(step - 2)).start()

        @pl.when((step >= 6) & (step < 9))
        def _():
            near(step - 6).wait_recv()
            swap(FAR + step - 6, near_source(step - 6)).start()

        @pl.when(step >= 3)
        def _():
            swap(step - 3, source(step - 3)).wait_recv()
            project(source(step - 3))

        @pl.when((step >= 8) & (step < 11))
        def _():
            swap(FAR + step - 8, near_source(step - 8)).wait_recv()
            project(near_source(step - 8))

    lane1 = lax.broadcasted_iota(jnp.int32, (1, 128), 1)
    bias = jnp.where(
        lane1 < 16,
        jnp.where(lane1 < 8, in_bias[0, 0], in_bias[1, 0]),
        jnp.where(lane1 < 24, forget_bias[0, 0], forget_bias[1, 0]),
    )
    pre = gates[...] + bias
    forget = pltpu.roll(jax.nn.log_sigmoid(pre), 112, 1)
    row = lax.broadcasted_iota(jnp.int32, (256, 256), 0)
    col = lax.broadcasted_iota(jnp.int32, (256, 256), 1)
    lower = jnp.where(col < row, 1.0, 0.0)
    before = jnp.dot(lower, forget, preferred_element_type=F32, precision=lax.Precision.HIGHEST)
    total = before[255:256, :] + forget[255:256, :]
    log_weight = pre + jnp.where(lane1 < 8, total - before - forget, before)
    stable = jnp.maximum(total, jnp.max(log_weight, axis=0, keepdims=True))
    weight = jnp.exp(log_weight - stable) * 128.0**-0.5
    stable_out[0:1, :] = stable[:, 0:8]
    stable_out[1:2, :] = pltpu.roll(stable, 120, 1)[:, 0:8]

    query_rows = query[...]
    numerators = []
    normals = ([], [])
    for b in range(8):
        float_keys = keys[b].astype(F32)
        float_values = values[b].astype(F32)
        weighted = []
        for g in range(2):
            spread_weight = jnp.broadcast_to(weight[:, 8 * g + b : 8 * g + b + 1], (256, 128))
            weighted.append((float_values * spread_weight).astype(BF16))
            normals[g].append(jnp.sum(float_keys * spread_weight, axis=0, keepdims=True))
        cells = lax.dot_general(
            keys[b], jnp.concatenate(weighted, axis=1), (((0,), (0,)), ((), ())), preferred_element_type=F32
        ).astype(BF16)
        memory_out[0, b] = cells[:, :128]
        memory_out[1, b] = cells[:, 128:]
        numerators.append(jnp.dot(query_rows, cells, preferred_element_type=F32)[b : b + 1])
    numerator = jnp.concatenate(numerators, axis=0)

    seq8 = lax.broadcasted_iota(jnp.int32, (8, 128), 0)
    lane8 = lax.broadcasted_iota(jnp.int32, (8, 128), 1)
    float_query = query_rows.astype(F32)
    hidden = jnp.zeros((8, 128), F32)
    for g in range(2):
        normal = jnp.concatenate(normals[g], axis=0)
        normal_out[g] = normal
        denominator = jnp.sum(float_query * normal, axis=1, keepdims=True)
        own_stable = jnp.sum(
            jnp.where(lane8 == 8 * g + seq8, jnp.broadcast_to(stable, (8, 128)), 0.0), axis=1, keepdims=True
        )
        floor_value = jnp.maximum(jnp.maximum(jnp.abs(denominator), jnp.exp(-own_stable)), 1.0)
        hidden = hidden + numerator[:, 128 * g : 128 * g + 128] / floor_value
    head_terms = jnp.dot(hidden.astype(BF16), out_w[...], preferred_element_type=F32)
    for t in range(8):
        terms[t] = head_terms[:, 128 * t : 128 * t + 128]

    me = 2 * x + c

    def term(k):
        tx, tc = lax.rem(x + k // 2, 4), lax.rem(c + lax.rem(k, 2), 2)
        return pltpu.make_async_remote_copy(
            src_ref=terms.at[2 * tx + tc],
            dst_ref=parts.at[k],
            send_sem=term_send.at[k],
            recv_sem=term_recv.at[k],
            device_id={"x": tx, "c": tc},
            device_id_type=MESH,
        )

    @pl.loop(1, 8)
    def _(k):
        term(k).start()

    @pl.loop(0, FAR)
    def _(k):
        far(k).wait_send()
        swap(k, source(k)).wait_send()
        for which in range(3):
            along_x(k, which).wait_send()

    @pl.loop(0, 3)
    def _(k):
        near(k).wait_send()
        swap(FAR + k, near_source(k)).wait_send()

    @pl.loop(1, 8)
    def _(k):
        term(k).wait_recv()

    total_read = terms[me]
    for k in range(1, 8):
        total_read = total_read + parts[k]
    read_out[...] = total_read.astype(BF16)

    @pl.loop(1, 8)
    def _(k):
        term(k).wait_send()


def shards(prompt, w_key, w_value, w_in_gate, w_forget_gate, in_bias, forget_bias, query, w_out):
    w_gate = jnp.concatenate(
        [w_in_gate[:, :, 0], w_forget_gate[:, :, 0], jnp.zeros((4, 1024), BF16)], axis=0
    )
    vmem = pl.BlockSpec(memory_space=pltpu.VMEM)
    smem = pl.BlockSpec(memory_space=pltpu.SMEM)
    anywhere = pl.BlockSpec(memory_space=pl.ANY)
    dma = pltpu.SemaphoreType.DMA
    memory, normal, stable, read = pl.pallas_call(
        kernel,
        out_shape=(
            jax.ShapeDtypeStruct((2, 8, 128, 128), BF16),
            jax.ShapeDtypeStruct((2, 8, 128), F32),
            jax.ShapeDtypeStruct((2, 8), F32),
            jax.ShapeDtypeStruct((8, 128), BF16),
        ),
        in_specs=[anywhere, anywhere, anywhere, vmem, smem, smem, vmem, anywhere],
        out_specs=(vmem, vmem, vmem, vmem),
        scratch_shapes=[
            pltpu.VMEM((16, 8, 16, 1024), BF16),
            pltpu.VMEM((1024, 256), BF16),
            pltpu.VMEM((1024, 128), BF16),
            pltpu.VMEM((128, 1024), BF16),
            pltpu.VMEM((8, 256, 128), BF16),
            pltpu.VMEM((8, 256, 128), BF16),
            pltpu.VMEM((256, 128), F32),
            pltpu.VMEM((8, 8, 128), F32),
            pltpu.VMEM((8, 8, 128), F32),
            dma((4,)),
            dma((FAR,)),
            dma((FAR,)),
            dma((3,)),
            dma((3,)),
            dma((FAR, 3)),
            dma((FAR, 3)),
            dma((FAR + 3,)),
            dma((FAR + 3,)),
            dma((8,)),
            dma((8,)),
        ],
        compiler_params=pltpu.CompilerParams(
            collective_id=0, has_side_effects=True, vmem_limit_bytes=32 * 1024 * 1024
        ),
    )(
        prompt, w_key[:, 0], w_value[:, 0], w_gate, in_bias, forget_bias, query[:, 0], w_out[0]
    )
    return memory[:, :, None], normal[:, :, None], stable[:, :, None], read


def solution(mesh):
    torus = Mesh(
        mesh.devices.reshape(mesh.shape["gr"], 4, 4, 4, 2), ("gr", "z", "y", "x", "c")
    )
    sp = ("z", "y")
    both = ("gr", "z", "y")
    return jax.shard_map(
        shards,
        mesh=torus,
        in_specs=(
            P("gr", sp, None),
            P(None, TP, None),
            P(None, TP, None),
            P(None, None, TP),
            P(None, None, TP),
            P(None, TP),
            P(None, TP),
            P(both, TP, None),
            P(TP, None, None),
        ),
        out_specs=(
            P(None, both, TP, None, None),
            P(None, both, TP, None),
            P(None, both, TP),
            P(both, TP),
        ),
        check_vma=False,
    )
```

time: 104 us -> 62.1 us (0.60)
  Pallas kernels: 0 us -> 50.6 us
  blocking collectives: 25.3 us -> 0 us
  starting transfers between devices: 23.3 us -> 0 us
  matrix products: 20.6 us -> 0 us
  waiting for transfers between devices: 20 us -> 0 us
  other arithmetic: 6.27 us -> 0.78 us
  local copies, waits for them, and re-layouts: 6.19 us -> 9.81 us
  between operations: 2.33 us -> 0.65 us
    pallas_call x0 -> x1, Pallas kernels: none -> 50.6 us  [shards(): pl.pallas_call(kernel, out_shape=(jax.ShapeDtypeStruct((2, 8, 128, 128),...]
    unnamed x3 -> x0, blocking collectives: 25.3 us -> none
    all_to_all x3 -> x0, starting transfers between devices: 23.3 us -> none  [the longest x1 9.18 us: shards(): lax.all_to_all(gate_values, 'sp', split_axis=0, concat_axis=1, tiled=True)]
    dot_general x7 -> x0, matrix products: 20.6 us -> none  [the longest x1 7.33 us: project(): jnp.einsum('bsd,gdh->bsgh', token_rows, w_forget_gate, preferred_element_...]
    all_to_all x3 -> x0, waiting for transfers between devices: 20 us -> none  [the longest x1 12.7 us: shards(): lax.all_to_all(value_rows, 'sp', split_axis=0, concat_axis=1, tiled=True)]
    unnamed x26 -> x16, local copies, waits for them, and re-layouts: 2.57 us -> 9.73 us
    another operation x6 -> x0, other arithmetic: 2.41 us -> none
    squeeze x4 -> x0, local copies, waits for them, and re-layouts: 1.46 us -> none  [the longest x2 1.3 us: sum_in_order(): return parts[0]]
  transfers between devices with their start and end apart: 3 -> 0, of which waited for: 2 -> 0; matrix products, arithmetic and copies ran while one was open for 14% -> 0% of each run, Pallas kernels for 0% -> 0%
where the time goes in v1:
time: 62.1 us; the launch traced here: 61.8 us
  Pallas kernels  50.6 us (81%)
  local copies, waits for them, and re-layouts  9.81 us (16%)
  other arithmetic  0.78 us (1%)
  between operations  0.65 us (1%)
    pallas_call x1, Pallas kernels, shards(): pl.pallas_call(kernel, out_shape=(jax.ShapeDtypeStruct((2, 8, 128, 128),...  50.6 us
    unnamed x16, local copies, waits for them, and re-layouts  9.73 us

profile of v1, /device:TPU:1, one launch (start us, length us, event | category | flops | bytes accessed | tf_op | source)
XLA Modules:
  0.0 61.8 jit_solution(9948238531359599849)
XLA Ops:
  0.6 0.1 pad.2.clone
  0.7 0.7 %copy.13.in_bias = f32[2,1]{1,0:T(2,128)S(1)} copy(f32[2,1]{0,1:T(1,128)} %param.14) | data formatting | bytes 16 | tf_op args[5]
  1.5 0.7 %copy.14.forget_bias = f32[2,1]{1,0:T(2,128)S(1)} copy(f32[2,1]{0,1:T(1,128)} %param.15) | data formatting | bytes 16 | tf_op args[6]
  2.2 0.8 %maximum_maximum_fusion.w_gate = bf16[8,1024]{1,0:T(8,128)(2,1)S(1)} fusion(bf16[2,1024]{1,0:T(2,128)(2,1)} %bitcast.22, bf16[2,1024]{1,0:T(2,128)(2,1)} %bitcast.23, bf16[8]{0:T(256)(128)(2,1)S(1)} %pad.2.clone), kind=kLoop, calls=%fused_computation | loop fusion | flops 49152 | bytes 24592 | tf_op jit(solution)/shard_map/concatenate | solution.py:276
  3.0 0.0 copy-start
  3.0 2.2 %copy-done = bf16[128,16,1024]{2,1,0:T(8,128)(2,1)S(1)} copy-done((bf16[128,16,1024]{2,1,0:T(8,128)(2,1)S(1)}, bf16[128,16,1024]{2,1,0:T(8,128)(2,1)}, u32[]{:S(2)}) %copy-start) | copy-done | bytes 4194328
  5.2 0.0 copy-start.1
  5.2 0.9 %copy-done.1 = bf16[1024,1,128]{2,0,1:T(8,128)(2,1)S(1)} copy-done((bf16[1024,1,128]{2,0,1:T(8,128)(2,1)S(1)}, bf16[1024,1,128]{2,0,1:T(8,128)(2,1)}, u32[]{:S(2)}) %copy-start.1) | copy-done | bytes 262168
  6.1 0.0 copy-start.2
  6.1 0.9 %copy-done.2 = bf16[1024,1,128]{2,0,1:T(8,128)(2,1)S(1)} copy-done((bf16[1024,1,128]{2,0,1:T(8,128)(2,1)S(1)}, bf16[1024,1,128]{2,0,1:T(8,128)(2,1)}, u32[]{:S(2)}) %copy-start.2) | copy-done | bytes 262168
  7.1 0.0 copy-start.3
  7.1 0.9 %copy-done.3 = bf16[1,128,1024]{2,1,0:T(8,128)(2,1)S(1)} copy-done((bf16[1,128,1024]{2,1,0:T(8,128)(2,1)S(1)}, bf16[1,128,1024]{2,1,0:T(8,128)(2,1)}, u32[]{:S(2)}) %copy-start.3) | copy-done | bytes 262168
  8.0 0.0 copy-start.4
  8.0 0.7 %copy-done.4 = bf16[8,1,128]{2,0,1:T(8,128)(2,1)S(1)} copy-done((bf16[8,1,128]{2,0,1:T(8,128)(2,1)S(1)}, bf16[8,1,128]{2,0,1:T(8,128)(2,1)}, u32[]{:S(2)}) %copy-start.4) | copy-done | bytes 2072
  8.7 50.6 %shard_map.120 = (bf16[2,8,128,128]{3,2,1,0:T(8,128)(2,1)S(1)}, f32[2,8,128]{2,1,0:T(8,128)S(1)}, f32[2,8]{1,0:T(2,128)S(1)}, bf16[8,128]{1,0:T(8,128)(2,1)S(1)}) custom-call(bf16[128,16,1024]{2,1,0:T(8,128)(2,1)S(1)} %copy-done, bf16[1024,128]{1,0:T(8,128)(2,1)S(1)} %bitcast.16, bf16[1024,128]{1,0:T(8,128)(2,1)S(1)} %bitcast.17, ...), custom_call_target="tpu_custom_call" | custom-call | tf_op jit(solution)/shard_map/pallas_call | solution.py:283
  59.3 0.8 %copy.22 = bf16[2,8,1,128,128]{4,3,2,1,0:T(8,128)(2,1)} copy(bf16[2,8,1,128,128]{4,3,2,1,0:T(8,128)(2,1)S(1)} %bitcast.15) | data formatting | bytes 1048576
  60.1 0.6 copy.23
  60.7 0.6 copy.24
  61.2 0.6 copy.25
  (1 shorter events, 0.0 us)
Async XLA Ops:
  3.0 2.2 %copy-start = (bf16[128,16,1024]{2,1,0:T(8,128)(2,1)S(1)}, bf16[128,16,1024]{2,1,0:T(8,128)(2,1)}, u32[]{:S(2)}) copy-start(bf16[128,16,1024]{2,1,0:T(8,128)(2,1)} %prompt.1) | copy-start | bytes 12582916
  5.2 0.9 %copy-start.1 = (bf16[1024,1,128]{2,0,1:T(8,128)(2,1)S(1)}, bf16[1024,1,128]{2,0,1:T(8,128)(2,1)}, u32[]{:S(2)}) copy-start(bf16[1024,1,128]{2,0,1:T(8,128)(2,1)} %param.10) | copy-start | bytes 786436
  6.1 0.9 %copy-start.2 = (bf16[1024,1,128]{2,0,1:T(8,128)(2,1)S(1)}, bf16[1024,1,128]{2,0,1:T(8,128)(2,1)}, u32[]{:S(2)}) copy-start(bf16[1024,1,128]{2,0,1:T(8,128)(2,1)} %param.11) | copy-start | bytes 786436
  7.1 0.9 %copy-start.3 = (bf16[1,128,1024]{2,1,0:T(8,128)(2,1)S(1)}, bf16[1,128,1024]{2,1,0:T(8,128)(2,1)}, u32[]{:S(2)}) copy-start(bf16[1,128,1024]{2,1,0:T(8,128)(2,1)} %param.17) | copy-start | bytes 786436
  8.0 0.7 %copy-start.4 = (bf16[8,1,128]{2,0,1:T(8,128)(2,1)S(1)}, bf16[8,1,128]{2,0,1:T(8,128)(2,1)}, u32[]{:S(2)}) copy-start(bf16[8,1,128]{2,0,1:T(8,128)(2,1)} %param.16) | copy-start | bytes 6148

commit v2 on v1

--- a/solution.py
+++ b/solution.py
@@ -20,9 +20,9 @@
 
 
 def kernel(
-    prompt, w_key, w_value, w_gate, in_bias, forget_bias, query, w_out,
+    prompt, w_key, w_value, w_in, w_forget, in_bias, forget_bias, query, w_out,
     memory_out, normal_out, stable_out, read_out,
-    rows, weights, gate_w, out_w, keys, values, gates, terms, parts,
+    rows, weights, gate_rows, gate_w, biases, queries, out_w, keys, values, gates, terms, parts,
     load_sem, far_send, far_recv, near_send, near_recv, x_send, x_recv, swap_send, swap_recv, term_send, term_recv,
 ):
     z, y, x, c = (lax.axis_index(a) for a in ("z", "y", "x", "c"))
@@ -36,7 +36,12 @@
         pltpu.make_async_copy(w_key, weights.at[:, pl.ds(0, 128)], load_sem.at[0]),
         pltpu.make_async_copy(w_value, weights.at[:, pl.ds(128, 128)], load_sem.at[1]),
         pltpu.make_async_copy(prompt.at[pl.ds(here * 8, 8)], rows.at[here], load_sem.at[2]),
-        pltpu.make_async_copy(w_out, out_w, load_sem.at[3]),
+        pltpu.make_async_copy(w_in, gate_rows.at[0], load_sem.at[3]),
+        pltpu.make_async_copy(w_forget, gate_rows.at[1], load_sem.at[4]),
+        pltpu.make_async_copy(in_bias, biases.at[pl.ds(0, 1)], load_sem.at[5]),
+        pltpu.make_async_copy(forget_bias, biases.at[pl.ds(1, 1)], load_sem.at[6]),
+        pltpu.make_async_copy(query, queries, load_sem.at[7]),
+        pltpu.make_async_copy(w_out, out_w, load_sem.at[8]),
     ]
     for load in loads:
         load.start()
@@ -116,12 +121,18 @@
     def _(k):
         near(k).start()
 
-    lane8 = lax.broadcasted_iota(jnp.int32, (8, 128), 1) // 8
-    gate8 = lax.broadcasted_iota(jnp.int32, (8, 128), 0)
-    spread = jnp.where(lane8 == gate8, 1.0, 0.0).astype(BF16)
-    gate_w[...] = lax.dot_general(
-        w_gate[...], spread, (((0,), (0,)), ((), ())), preferred_element_type=F32
-    ).astype(BF16)
+    for load in loads:
+        load.wait()
+
+    lane_gate = lax.broadcasted_iota(jnp.int32, (2, 128), 1) // 8
+    gate2 = lax.broadcasted_iota(jnp.int32, (2, 128), 0)
+    spread_gates = 0.0
+    for kind in range(2):
+        spread = jnp.where(lane_gate == 2 * kind + gate2, 1.0, 0.0).astype(BF16)
+        spread_gates = spread_gates + lax.dot_general(
+            gate_rows[kind], spread, (((0,), (0,)), ((), ())), preferred_element_type=F32
+        )
+    gate_w[...] = spread_gates.astype(BF16)
 
     lane = lax.broadcasted_iota(jnp.int32, (8, 16, 128), 2)
     which_seq = lax.broadcasted_iota(jnp.int32, (8, 16, 128), 0)
@@ -136,8 +147,6 @@
         pre = jnp.dot(block, gate_w[...], preferred_element_type=F32).reshape(8, 16, 128)
         gates[at, :] = jnp.sum(jnp.where(own_lane, pre, 0.0), axis=0)
 
-    for load in loads:
-        load.wait()
     project(here)
 
     @pl.loop(0, FAR + 3)
@@ -177,8 +186,8 @@
     lane1 = lax.broadcasted_iota(jnp.int32, (1, 128), 1)
     bias = jnp.where(
         lane1 < 16,
-        jnp.where(lane1 < 8, in_bias[0, 0], in_bias[1, 0]),
-        jnp.where(lane1 < 24, forget_bias[0, 0], forget_bias[1, 0]),
+        jnp.where(lane1 < 8, biases[0:1, 0:1], biases[0:1, 1:2]),
+        jnp.where(lane1 < 24, biases[1:2, 0:1], biases[1:2, 1:2]),
     )
     pre = gates[...] + bias
     forget = pltpu.roll(jax.nn.log_sigmoid(pre), 112, 1)
@@ -193,7 +202,7 @@
     stable_out[0:1, :] = stable[:, 0:8]
     stable_out[1:2, :] = pltpu.roll(stable, 120, 1)[:, 0:8]
 
-    query_rows = query[...]
+    query_rows = queries[...]
     numerators = []
     normals = ([], [])
     for b in range(8):
@@ -273,12 +282,8 @@
 
 
 def shards(prompt, w_key, w_value, w_in_gate, w_forget_gate, in_bias, forget_bias, query, w_out):
-    w_gate = jnp.concatenate(
-        [w_in_gate[:, :, 0], w_forget_gate[:, :, 0], jnp.zeros((4, 1024), BF16)], axis=0
-    )
     vmem = pl.BlockSpec(memory_space=pltpu.VMEM)
-    smem = pl.BlockSpec(memory_space=pltpu.SMEM)
-    anywhere = pl.BlockSpec(memory_space=pl.ANY)
+    hbm = pl.BlockSpec(memory_space=pltpu.HBM)
     dma = pltpu.SemaphoreType.DMA
     memory, normal, stable, read = pl.pallas_call(
         kernel,
@@ -288,19 +293,22 @@
             jax.ShapeDtypeStruct((2, 8), F32),
             jax.ShapeDtypeStruct((8, 128), BF16),
         ),
-        in_specs=[anywhere, anywhere, anywhere, vmem, smem, smem, vmem, anywhere],
+        in_specs=[hbm] * 9,
         out_specs=(vmem, vmem, vmem, vmem),
         scratch_shapes=[
             pltpu.VMEM((16, 8, 16, 1024), BF16),
             pltpu.VMEM((1024, 256), BF16),
+            pltpu.VMEM((2, 2, 1024), BF16),
             pltpu.VMEM((1024, 128), BF16),
+            pltpu.VMEM((2, 2), F32),
+            pltpu.VMEM((8, 128), BF16),
             pltpu.VMEM((128, 1024), BF16),
             pltpu.VMEM((8, 256, 128), BF16),
             pltpu.VMEM((8, 256, 128), BF16),
             pltpu.VMEM((256, 128), F32),
             pltpu.VMEM((8, 8, 128), F32),
             pltpu.VMEM((8, 8, 128), F32),
-            dma((4,)),
+            dma((9,)),
             dma((FAR,)),
             dma((FAR,)),
             dma((3,)),
@@ -313,10 +321,11 @@
             dma((8,)),
         ],
         compiler_params=pltpu.CompilerParams(
-            collective_id=0, has_side_effects=True, vmem_limit_bytes=32 * 1024 * 1024
+            collective_id=0, has_side_effects=True, vmem_limit_bytes=60 * 1024 * 1024
         ),
     )(
-        prompt, w_key[:, 0], w_value[:, 0], w_gate, in_bias, forget_bias, query[:, 0], w_out[0]
+        prompt, w_key[:, 0], w_value[:, 0], w_in_gate[:, :, 0], w_forget_gate[:, :, 0],
+        in_bias.T, forget_bias.T, query[:, 0], w_out[0],
     )
     return memory[:, :, None], normal[:, :, None], stable[:, :, None], read
 

time: 62.1 us -> 57.5 us (0.926)
  local copies, waits for them, and re-layouts: 9.81 us -> 5.62 us
  other arithmetic: 0.78 us -> 0 us
    unnamed x16 -> x4, local copies, waits for them, and re-layouts: 9.73 us -> 5.62 us
    concatenate x1 -> x0, other arithmetic: 0.78 us -> none  [shards(): jnp.concatenate([w_in_gate[:, :, 0], w_forget_gate[:, :, 0], jnp.zeros((4...]
where the time goes in v2:
time: 57.5 us; the launch traced here: 57.3 us
  Pallas kernels  51 us (89%)
  local copies, waits for them, and re-layouts  5.62 us (10%)
  between operations  0.64 us (1%)
    pallas_call x1, Pallas kernels, shards(): pl.pallas_call(kernel, out_shape=(jax.ShapeDtypeStruct((2, 8, 128, 128),...  51 us
    unnamed x4, local copies, waits for them, and re-layouts  5.62 us

profile of v2, /device:TPU:1, one launch (start us, length us, event | category | flops | bytes accessed | tf_op | source)
XLA Modules:
  0.0 57.3 jit_solution(7955044684777512847)
XLA Ops:
  0.6 51.0 %shard_map.120 = (bf16[2,8,128,128]{3,2,1,0:T(8,128)(2,1)}, f32[2,8,128]{2,1,0:T(8,128)}, f32[2,8]{1,0:T(2,128)}, bf16[8,128]{1,0:T(8,128)(2,1)}) custom-call(bf16[128,16,1024]{2,1,0:T(8,128)(2,1)} %prompt.1, bf16[1024,128]{1,0:T(8,128)(2,1)} %bitcast.18, bf16[1024,128]{1,0:T(8,128)(2,1)} %bitcast.19, bf16[2,1024]{1,0:T(2,128)(2,1)} %bitcast.22, ...), custom_call_target="tpu_custom_call" | custom-call | tf_op jit(solution)/shard_map/pallas_call | solution.py:288
  51.7 1.9 %copy.20 = bf16[2,8,1,128,128]{4,3,2,1,0:T(8,128)(2,1)} copy(bf16[2,8,1,128,128]{4,3,2,1,0:T(8,128)(2,1)} %bitcast.17) | data formatting | bytes 1048576
  53.6 1.3 %copy.21 = f32[2,8,1,128]{3,2,1,0:T(1,128)} copy(f32[2,8,1,128]{3,2,1,0:T(1,128)} %bitcast.21) | data formatting | bytes 16384
  54.9 1.2 %copy.22 = f32[2,8,1]{1,2,0:T(1,128)} copy(f32[2,8,1]{1,2,0:T(1,128)} %bitcast.25) | data formatting | bytes 128
  56.1 1.2 %copy.23 = bf16[8,128]{1,0:T(8,128)(2,1)} copy(bf16[8,128]{1,0:T(8,128)(2,1)} %get-tuple-element.23) | data formatting | bytes 4096

commit v3 on v2

--- a/solution.py
+++ b/solution.py
@@ -22,7 +22,7 @@
 def kernel(
     prompt, w_key, w_value, w_in, w_forget, in_bias, forget_bias, query, w_out,
     memory_out, normal_out, stable_out, read_out,
-    rows, weights, gate_rows, gate_w, biases, queries, out_w, keys, values, gates, terms, parts,
+    rows, weights, gate_rows, gate_w, biases, queries, query_w, out_w, keys, values, gates, scores, terms, parts,
     load_sem, far_send, far_recv, near_send, near_recv, x_send, x_recv, swap_send, swap_recv, term_send, term_recv,
 ):
     z, y, x, c = (lax.axis_index(a) for a in ("z", "y", "x", "c"))
@@ -72,8 +72,11 @@
             device_id_type=MESH,
         )
 
+    def near_offset(k):
+        return lax.rem(2 * k + 1 - k // 2 * 3, 4)
+
     def near(k):
-        ty = lax.rem(y + k + 1, 4)
+        ty = lax.rem(y + near_offset(k), 4)
         return pltpu.make_async_remote_copy(
             src_ref=prompt.at[pl.ds((z * 4 + ty) * 8 + 4 * c, 4)],
             dst_ref=rows.at[here, pl.ds(4 * c, 4)],
@@ -88,7 +91,7 @@
         return lax.rem(z + 4 - dz, 4) * 4 + lax.rem(y + 4 - dy, 4)
 
     def near_source(k):
-        return z * 4 + lax.rem(y + 3 - k, 4)
+        return z * 4 + lax.rem(y + 4 - near_offset(k), 4)
 
     def along_x(k, which):
         held = seq if which < 2 else 4 * c + down
@@ -113,13 +116,13 @@
             device_id_type=MESH,
         )
 
-    @pl.loop(0, FAR)
+    @pl.loop(0, 12)
     def _(k):
         far(k).start()
 
-    @pl.loop(0, 3)
-    def _(k):
-        near(k).start()
+    near(0).start()
+    near(1).start()
+    near(2).start()
 
     for load in loads:
         load.wait()
@@ -134,6 +137,12 @@
         )
     gate_w[...] = spread_gates.astype(BF16)
 
+    lane8 = lax.broadcasted_iota(jnp.int32, (8, 128), 1)
+    pick = jnp.where(lax.rem(lane8, 8) == lax.broadcasted_iota(jnp.int32, (8, 128), 0), 1.0, 0.0)
+    query_w[...] = lax.dot_general(
+        queries[...], pick.astype(BF16), (((0,), (0,)), ((), ())), preferred_element_type=F32
+    ).astype(BF16)
+
     lane = lax.broadcasted_iota(jnp.int32, (8, 16, 128), 2)
     which_seq = lax.broadcasted_iota(jnp.int32, (8, 16, 128), 0)
     own_lane = lax.rem(lane, 8) == which_seq
@@ -142,14 +151,17 @@
         block = rows[src].reshape(128, 1024)
         both = jnp.dot(block, weights[...], preferred_element_type=F32)
         at = pl.ds(pl.multiple_of(src * 16, 16), 16)
-        keys[:, at, :] = both[:, :128].astype(BF16).reshape(8, 16, 128)
+        key_rows = both[:, :128].astype(BF16)
+        keys[:, at, :] = key_rows.reshape(8, 16, 128)
         values[:, at, :] = both[:, 128:].astype(BF16).reshape(8, 16, 128)
         pre = jnp.dot(block, gate_w[...], preferred_element_type=F32).reshape(8, 16, 128)
         gates[at, :] = jnp.sum(jnp.where(own_lane, pre, 0.0), axis=0)
+        score = jnp.dot(key_rows, query_w[...], preferred_element_type=F32).reshape(8, 16, 128)
+        scores[at, :] = jnp.sum(jnp.where(own_lane, score, 0.0), axis=0)
 
     project(here)
 
-    @pl.loop(0, FAR + 3)
+    @pl.loop(0, FAR + 10)
     def _(step):
         @pl.when(step < FAR)
         def _():
@@ -157,31 +169,31 @@
             along_x(step, 0).start()
             along_x(step, 1).start()
 
-        @pl.when((step >= 1) & (step < FAR + 1))
-        def _():
-            along_x(step - 1, 0).wait_recv()
-            along_x(step - 1, 2).start()
-
-        @pl.when((step >= 2) & (step < FAR + 2))
-        def _():
-            along_x(step - 2, 1).wait_recv()
-            along_x(step - 2, 2).wait_recv()
-            swap(step - 2, source(step - 2)).start()
+        @pl.when((step >= 4) & (step < FAR + 4))
+        def _():
+            along_x(step - 4, 0).wait_recv()
+            along_x(step - 4, 2).start()
+
+        @pl.when((step >= 8) & (step < FAR + 8))
+        def _():
+            along_x(step - 8, 1).wait_recv()
+            along_x(step - 8, 2).wait_recv()
+            swap(step - 8, source(step - 8)).start()
 
         @pl.when((step >= 6) & (step < 9))
         def _():
             near(step - 6).wait_recv()
             swap(FAR + step - 6, near_source(step - 6)).start()
 
-        @pl.when(step >= 3)
-        def _():
-            swap(step - 3, source(step - 3)).wait_recv()
-            project(source(step - 3))
-
-        @pl.when((step >= 8) & (step < 11))
-        def _():
-            swap(FAR + step - 8, near_source(step - 8)).wait_recv()
-            project(near_source(step - 8))
+        @pl.when(step >= 10)
+        def _():
+            swap(step - 10, source(step - 10)).wait_recv()
+            project(source(step - 10))
+
+        @pl.when((step >= 9) & (step < 12))
+        def _():
+            swap(FAR + step - 9, near_source(step - 9)).wait_recv()
+            project(near_source(step - 9))
 
     lane1 = lax.broadcasted_iota(jnp.int32, (1, 128), 1)
     bias = jnp.where(
@@ -202,9 +214,40 @@
     stable_out[0:1, :] = stable[:, 0:8]
     stable_out[1:2, :] = pltpu.roll(stable, 120, 1)[:, 0:8]
 
-    query_rows = queries[...]
-    numerators = []
-    normals = ([], [])
+    read_weight = weight * scores[...]
+    denominator = jnp.sum(read_weight, axis=0, keepdims=True)
+    floor_value = jnp.maximum(jnp.maximum(jnp.abs(denominator), jnp.exp(-stable)), 1.0)
+    read_weight = read_weight / floor_value
+    read_weight = read_weight + pltpu.roll(read_weight, 120, 1)
+    by_seq = read_weight.T[0:8]
+    high = by_seq.astype(BF16)
+    both_parts = jnp.concatenate([high.astype(F32), by_seq - high.astype(F32)], axis=0).astype(BF16)
+    hidden = []
+    for b in range(8):
+        two = jnp.dot(both_parts, values[b], preferred_element_type=F32)
+        hidden.append(two[b : b + 1] + two[8 + b : 9 + b])
+    hidden = jnp.concatenate(hidden, axis=0).astype(BF16)
+    head_terms = jnp.dot(hidden, out_w[...], preferred_element_type=F32)
+    for t in range(8):
+        terms[t] = head_terms[:, 128 * t : 128 * t + 128]
+
+    me = 2 * x + c
+
+    def term(k):
+        tx, tc = lax.rem(x + k // 2, 4), lax.rem(c + lax.rem(k, 2), 2)
+        return pltpu.make_async_remote_copy(
+            src_ref=terms.at[2 * tx + tc],
+            dst_ref=parts.at[k],
+            send_sem=term_send.at[k],
+            recv_sem=term_recv.at[k],
+            device_id={"x": tx, "c": tc},
+            device_id_type=MESH,
+        )
+
+    @pl.loop(1, 8)
+    def _(k):
+        term(k).start()
+
     for b in range(8):
         float_keys = keys[b].astype(F32)
         float_values = values[b].astype(F32)
@@ -212,48 +255,12 @@
         for g in range(2):
             spread_weight = jnp.broadcast_to(weight[:, 8 * g + b : 8 * g + b + 1], (256, 128))
             weighted.append((float_values * spread_weight).astype(BF16))
-            normals[g].append(jnp.sum(float_keys * spread_weight, axis=0, keepdims=True))
+            normal_out[g, b : b + 1, :] = jnp.sum(float_keys * spread_weight, axis=0, keepdims=True)
         cells = lax.dot_general(
             keys[b], jnp.concatenate(weighted, axis=1), (((0,), (0,)), ((), ())), preferred_element_type=F32
         ).astype(BF16)
         memory_out[0, b] = cells[:, :128]
         memory_out[1, b] = cells[:, 128:]
-        numerators.append(jnp.dot(query_rows, cells, preferred_element_type=F32)[b : b + 1])
-    numerator = jnp.concatenate(numerators, axis=0)
-
-    seq8 = lax.broadcasted_iota(jnp.int32, (8, 128), 0)
-    lane8 = lax.broadcasted_iota(jnp.int32, (8, 128), 1)
-    float_query = query_rows.astype(F32)
-    hidden = jnp.zeros((8, 128), F32)
-    for g in range(2):
-        normal = jnp.concatenate(normals[g], axis=0)
-        normal_out[g] = normal
-        denominator = jnp.sum(float_query * normal, axis=1, keepdims=True)
-        own_stable = jnp.sum(
-            jnp.where(lane8 == 8 * g + seq8, jnp.broadcast_to(stable, (8, 128)), 0.0), axis=1, keepdims=True
-        )
-        floor_value = jnp.maximum(jnp.maximum(jnp.abs(denominator), jnp.exp(-own_stable)), 1.0)
-        hidden = hidden + numerator[:, 128 * g : 128 * g + 128] / floor_value
-    head_terms = jnp.dot(hidden.astype(BF16), out_w[...], preferred_element_type=F32)
-    for t in range(8):
-        terms[t] = head_terms[:, 128 * t : 128 * t + 128]
-
-    me = 2 * x + c
-
-    def term(k):
-        tx, tc = lax.rem(x + k // 2, 4), lax.rem(c + lax.rem(k, 2), 2)
-        return pltpu.make_async_remote_copy(
-            src_ref=terms.at[2 * tx + tc],
-            dst_ref=parts.at[k],
-            send_sem=term_send.at[k],
-            recv_sem=term_recv.at[k],
-            device_id={"x": tx, "c": tc},
-            device_id_type=MESH,
-        )
-
-    @pl.loop(1, 8)
-    def _(k):
-        term(k).start()
 
     @pl.loop(0, FAR)
     def _(k):
@@ -279,6 +286,15 @@
     @pl.loop(1, 8)
     def _(k):
         term(k).wait_send()
+
+
+def write_out(memory, normal, stable, read, memory_out, normal_out, stable_out, read_out, sems):
+    pairs = ((memory, memory_out), (normal, normal_out), (stable, stable_out), (read, read_out))
+    copies = [pltpu.make_async_copy(a, b, sems.at[k]) for k, (a, b) in enumerate(pairs)]
+    for copy in copies:
+        copy.start()
+    for copy in copies:
+        copy.wait()
 
 
 def shards(prompt, w_key, w_value, w_in_gate, w_forget_gate, in_bias, forget_bias, query, w_out):
@@ -302,9 +318,11 @@
             pltpu.VMEM((1024, 128), BF16),
             pltpu.VMEM((2, 2), F32),
             pltpu.VMEM((8, 128), BF16),
+            pltpu.VMEM((128, 128), BF16),
             pltpu.VMEM((128, 1024), BF16),
             pltpu.VMEM((8, 256, 128), BF16),
             pltpu.VMEM((8, 256, 128), BF16),
+            pltpu.VMEM((256, 128), F32),
             pltpu.VMEM((256, 128), F32),
             pltpu.VMEM((8, 8, 128), F32),
             pltpu.VMEM((8, 8, 128), F32),
@@ -321,12 +339,22 @@
             dma((8,)),
         ],
         compiler_params=pltpu.CompilerParams(
-            collective_id=0, has_side_effects=True, vmem_limit_bytes=60 * 1024 * 1024
+            collective_id=0, has_side_effects=True, vmem_limit_bytes=20 * 1024 * 1024
         ),
     )(
-        prompt, w_key[:, 0], w_value[:, 0], w_in_gate[:, :, 0], w_forget_gate[:, :, 0],
-        in_bias.T, forget_bias.T, query[:, 0], w_out[0],
+        *(pltpu.with_memory_space_constraint(v, pltpu.HBM) for v in (
+            prompt, w_key[:, 0], w_value[:, 0], w_in_gate[:, :, 0], w_forget_gate[:, :, 0],
+            in_bias.T, forget_bias.T, query[:, 0], w_out[0],
+        ))
     )
+    memory, normal, stable, read = pl.pallas_call(
+        write_out,
+        out_shape=tuple(jax.ShapeDtypeStruct(v.shape, v.dtype) for v in (memory, normal, stable, read)),
+        in_specs=[vmem] * 4,
+        out_specs=(hbm,) * 4,
+        scratch_shapes=[dma((4,))],
+        compiler_params=pltpu.CompilerParams(vmem_limit_bytes=4 * 1024 * 1024),
+    )(memory, normal, stable, read)
     return memory[:, :, None], normal[:, :, None], stable[:, :, None], read
 
 

time: 57.5 us -> 41.8 us (0.73)
  Pallas kernels: 51 us -> 41.1 us
  local copies, waits for them, and re-layouts: 5.62 us -> 0 us
    pallas_call x1, Pallas kernels: 51 us -> 40.2 us  [shards(): pl.pallas_call(kernel, out_shape=(jax.ShapeDtypeStruct((2, 8, 128, 128),...]
    unnamed x4 -> x0, local copies, waits for them, and re-layouts: 5.62 us -> none
    pallas_call x0 -> x1, Pallas kernels: none -> 0.84 us  [shards(): pl.pallas_call(write_out, out_shape=tuple((jax.ShapeDtypeStruct(v.shape,...]
where the time goes in v3:
time: 41.8 us; the launch traced here: 41.7 us
  Pallas kernels  41.1 us (98%)
  between operations  0.64 us (2%)
    pallas_call x1, Pallas kernels, shards(): pl.pallas_call(kernel, out_shape=(jax.ShapeDtypeStruct((2, 8, 128, 128),...  40.2 us
    pallas_call x1, Pallas kernels, shards(): pl.pallas_call(write_out, out_shape=tuple((jax.ShapeDtypeStruct(v.shape,...  0.84 us

profile of v3, /device:TPU:1, one launch (start us, length us, event | category | flops | bytes accessed | tf_op | source)
XLA Modules:
  0.0 41.7 jit_solution(12301074891523835252)
XLA Ops:
  0.6 40.2 %shard_map.120 = (bf16[2,8,128,128]{3,2,1,0:T(8,128)(2,1)S(1)}, f32[2,8,128]{2,1,0:T(8,128)S(1)}, f32[2,8]{1,0:T(2,128)S(1)}, bf16[8,128]{1,0:T(8,128)(2,1)S(1)}) custom-call(bf16[128,16,1024]{2,1,0:T(8,128)(2,1)} %prompt.1, bf16[1024,128]{1,0:T(8,128)(2,1)} %bitcast.17, bf16[1024,128]{1,0:T(8,128)(2,1)} %bitcast.18, bf16[2,1024]{1,0:T(2,128)(2,1)} %bitcast.20, ...), custom_call_target="tpu_custom_call" | custom-call | tf_op jit(solution)/shard_map/pallas_call | solution.py:304
  40.9 0.8 %shard_map.121 = (bf16[2,8,128,128]{3,2,1,0:T(8,128)(2,1)}, f32[2,8,128]{2,1,0:T(8,128)}, f32[2,8]{1,0:T(2,128)}, bf16[8,128]{1,0:T(8,128)(2,1)}) custom-call(bf16[2,8,128,128]{3,2,1,0:T(8,128)(2,1)S(1)} %get-tuple-element.12.memory, f32[2,8,128]{2,1,0:T(8,128)S(1)} %get-tuple-element.13.normal, f32[2,8]{1,0:T(2,128)S(1)} %get-tuple-element.14.stable, ...), custom_call_target="tpu_custom_call" | custom-call | tf_op jit(solution)/shard_map/pallas_call | solution.py:350

commit v4 on v3

--- a/solution.py
+++ b/solution.py
@@ -15,22 +15,26 @@
 FAR = 12
 
 
-def offsets(k):
-    return lax.rem(k, 3) + 1, k // 3
+OFFSETS = [(1, 0), (2, 0), (3, 0), (1, 1), (2, 1), (3, 1), (1, 3), (2, 3), (3, 3), (1, 2), (2, 2), (3, 2)]
+DIRECT = FAR - 12
+NEAR = (1, 3, 2)
 
 
 def kernel(
     prompt, w_key, w_value, w_in, w_forget, in_bias, forget_bias, query, w_out,
     memory_out, normal_out, stable_out, read_out,
     rows, weights, gate_rows, gate_w, biases, queries, query_w, out_w, keys, values, gates, scores, terms, parts,
-    load_sem, far_send, far_recv, near_send, near_recv, x_send, x_recv, swap_send, swap_recv, term_send, term_recv,
+    load_sem, far_send, far_recv, line_in, near_send, near_recv, x_send, x_recv, swap_send, swap_recv, term_send, term_recv,
 ):
     z, y, x, c = (lax.axis_index(a) for a in ("z", "y", "x", "c"))
     here = z * 4 + y
+    zs = [z] + [lax.rem(z + k, 4) for k in range(1, 4)]
+    ys = [y] + [lax.rem(y + k, 4) for k in range(1, 4)]
+    xs = [x] + [lax.rem(x + k, 4) for k in range(1, 4)]
+    cs = [c, 1 - c]
     seq = 4 * c + x
     up = lax.rem(x + 1 + 2 * c, 4)
     down = lax.rem(x + 3 + 2 * c, 4)
-    across = lax.rem(x + 2, 4)
 
     loads = [
         pltpu.make_async_copy(w_key, weights.at[:, pl.ds(0, 128)], load_sem.at[0]),
@@ -48,21 +52,18 @@
 
     barrier = pltpu.get_barrier_semaphore()
 
-    @pl.loop(1, 16)
-    def _(k):
-        to = {"z": lax.rem(z + k // 4, 4), "y": lax.rem(y + lax.rem(k, 4), 4)}
+    for k in range(3, 0, -1):
+        pl.semaphore_signal(barrier, inc=1, device_id={"z": zs[k]}, device_id_type=MESH)
+        pl.semaphore_signal(barrier, inc=1, device_id={"y": ys[k]}, device_id_type=MESH)
+    for k in range(7, 0, -1):
+        to = {"x": xs[k // 2], "c": cs[k % 2]}
         pl.semaphore_signal(barrier, inc=1, device_id=to, device_id_type=MESH)
 
-    @pl.loop(1, 8)
-    def _(k):
-        to = {"x": lax.rem(x + k // 2, 4), "c": lax.rem(c + lax.rem(k, 2), 2)}
-        pl.semaphore_signal(barrier, inc=1, device_id=to, device_id_type=MESH)
-
-    pl.semaphore_wait(barrier, 22)
+    pl.semaphore_wait(barrier, 13)
 
     def far(k):
-        dz, dy = offsets(k)
-        tz, ty = lax.rem(z + dz, 4), lax.rem(y + dy, 4)
+        dz, dy = OFFSETS[k]
+        tz, ty = zs[dz], ys[dy]
         return pltpu.make_async_remote_copy(
             src_ref=prompt.at[(tz * 4 + ty) * 8 + seq],
             dst_ref=rows.at[here, seq],
@@ -72,11 +73,8 @@
             device_id_type=MESH,
         )
 
-    def near_offset(k):
-        return lax.rem(2 * k + 1 - k // 2 * 3, 4)
-
     def near(k):
-        ty = lax.rem(y + near_offset(k), 4)
+        ty = ys[NEAR[k]]
         return pltpu.make_async_remote_copy(
             src_ref=prompt.at[pl.ds((z * 4 + ty) * 8 + 4 * c, 4)],
             dst_ref=rows.at[here, pl.ds(4 * c, 4)],
@@ -87,21 +85,21 @@
         )
 
     def source(k):
-        dz, dy = offsets(k)
-        return lax.rem(z + 4 - dz, 4) * 4 + lax.rem(y + 4 - dy, 4)
+        dz, dy = OFFSETS[k]
+        return zs[-dz] * 4 + ys[-dy]
 
     def near_source(k):
-        return z * 4 + lax.rem(y + 4 - near_offset(k), 4)
+        return z * 4 + ys[4 - NEAR[k]]
 
     def along_x(k, which):
-        held = seq if which < 2 else 4 * c + down
-        block = rows.at[source(k), held]
+        direct = k >= DIRECT
+        block = rows.at[source(k), seq if which < 2 or direct else 4 * c + down]
         return pltpu.make_async_remote_copy(
             src_ref=block,
             dst_ref=block,
             send_sem=x_send.at[k, which],
             recv_sem=x_recv.at[k, which],
-            device_id={"x": down if which == 1 else up},
+            device_id={"x": (up, down, xs[2] if direct else up)[which]},
             device_id_type=MESH,
         )
 
@@ -112,17 +110,14 @@
             dst_ref=block,
             send_sem=swap_send.at[k],
             recv_sem=swap_recv.at[k],
-            device_id={"c": 1 - c},
-            device_id_type=MESH,
-        )
-
-    @pl.loop(0, 12)
-    def _(k):
+            device_id={"c": cs[1]},
+            device_id_type=MESH,
+        )
+
+    for k in range(3, 0, -1):
+        pl.semaphore_signal(line_in, inc=1, device_id={"y": ys[k]}, device_id_type=MESH)
+    for k in range(3):
         far(k).start()
-
-    near(0).start()
-    near(1).start()
-    near(2).start()
 
     for load in loads:
         load.wait()
@@ -160,40 +155,59 @@
         scores[at, :] = jnp.sum(jnp.where(own_lane, score, 0.0), axis=0)
 
     project(here)
-
-    @pl.loop(0, FAR + 10)
-    def _(step):
-        @pl.when(step < FAR)
-        def _():
-            far(step).wait_recv()
-            along_x(step, 0).start()
-            along_x(step, 1).start()
-
-        @pl.when((step >= 4) & (step < FAR + 4))
-        def _():
-            along_x(step - 4, 0).wait_recv()
-            along_x(step - 4, 2).start()
-
-        @pl.when((step >= 8) & (step < FAR + 8))
-        def _():
-            along_x(step - 8, 1).wait_recv()
-            along_x(step - 8, 2).wait_recv()
-            swap(step - 8, source(step - 8)).start()
-
-        @pl.when((step >= 6) & (step < 9))
-        def _():
-            near(step - 6).wait_recv()
-            swap(FAR + step - 6, near_source(step - 6)).start()
-
-        @pl.when(step >= 10)
-        def _():
-            swap(step - 10, source(step - 10)).wait_recv()
-            project(source(step - 10))
-
-        @pl.when((step >= 9) & (step < 12))
-        def _():
-            swap(FAR + step - 9, near_source(step - 9)).wait_recv()
-            project(near_source(step - 9))
+    pl.semaphore_wait(line_in, 3)
+    for k in range(3, 4):
+        far(k).start()
+
+    def arrive(k):
+        far(k).wait_recv()
+        along_x(k, 0).start()
+        along_x(k, 1).start()
+        if k >= DIRECT:
+            along_x(k, 2).start()
+        if k + 4 < FAR:
+            far(k + 4).start()
+
+    def relay(k):
+        along_x(k, 0).wait_recv()
+        along_x(k, 2).start()
+
+    def start_swap(k):
+        if k >= DIRECT:
+            along_x(k, 0).wait_recv()
+        along_x(k, 1).wait_recv()
+        along_x(k, 2).wait_recv()
+        swap(k, source(k)).start()
+
+    def finish(k):
+        swap(k, source(k)).wait_recv()
+        project(source(k))
+
+    def start_near(k):
+        near(k).start()
+
+    def swap_near(k):
+        near(k).wait_recv()
+        swap(FAR + k, near_source(k)).start()
+
+    def finish_near(k):
+        swap(FAR + k, near_source(k)).wait_recv()
+        project(near_source(k))
+
+    events = []
+    for k in range(FAR):
+        events.append((k, 0, arrive, k))
+        if k < DIRECT:
+            events.append((k + 3, 2, relay, k))
+        events.append((k + 8, 3, start_swap, k))
+        events.append((k + 10, 4, finish, k))
+    for k in range(3):
+        if (2, 2, 4)[k]:
+            events.append(((2, 2, 4)[k], 5, start_near, k))
+        events.append(((6, 8, 10)[k], 6, swap_near, k))
+        events.append(((9, 11, 13)[k], 7, finish_near, k))
+    for _, _, stage, k in sorted(events, key=lambda e: (e[0], e[1], e[3])):
+        stage(k)
 
     lane1 = lax.broadcasted_iota(jnp.int32, (1, 128), 1)
     bias = jnp.where(
@@ -234,7 +248,7 @@
     me = 2 * x + c
 
     def term(k):
-        tx, tc = lax.rem(x + k // 2, 4), lax.rem(c + lax.rem(k, 2), 2)
+        tx, tc = xs[k // 2], cs[k % 2]
         return pltpu.make_async_remote_copy(
             src_ref=terms.at[2 * tx + tc],
             dst_ref=parts.at[k],
@@ -244,8 +258,7 @@
             device_id_type=MESH,
         )
 
-    @pl.loop(1, 8)
-    def _(k):
+    for k in range(1, 8):
         term(k).start()
 
     for b in range(8):
@@ -262,20 +275,17 @@
         memory_out[0, b] = cells[:, :128]
         memory_out[1, b] = cells[:, 128:]
 
-    @pl.loop(0, FAR)
-    def _(k):
+    for k in range(FAR):
         far(k).wait_send()
         swap(k, source(k)).wait_send()
         for which in range(3):
             along_x(k, which).wait_send()
 
-    @pl.loop(0, 3)
-    def _(k):
+    for k in range(3):
         near(k).wait_send()
         swap(FAR + k, near_source(k)).wait_send()
 
-    @pl.loop(1, 8)
-    def _(k):
+    for k in range(1, 8):
         term(k).wait_recv()
 
     total_read = terms[me]
@@ -283,8 +293,7 @@
         total_read = total_read + parts[k]
     read_out[...] = total_read.astype(BF16)
 
-    @pl.loop(1, 8)
-    def _(k):
+    for k in range(1, 8):
         term(k).wait_send()
 
 
@@ -329,6 +338,7 @@
             dma((9,)),
             dma((FAR,)),
             dma((FAR,)),
+            pltpu.SemaphoreType.REGULAR,
             dma((3,)),
             dma((3,)),
             dma((FAR, 3)),

time: 41.8 us -> 38.9 us (0.931)
  Pallas kernels: 41.1 us -> 38.2 us
    pallas_call x1, Pallas kernels: 40.2 us -> 37.3 us  [shards(): pl.pallas_call(kernel, out_shape=(jax.ShapeDtypeStruct((2, 8, 128, 128),...]
where the time goes in v4:
time: 38.9 us; the launch traced here: 38.8 us
  Pallas kernels  38.2 us (98%)
  between operations  0.64 us (2%)
    pallas_call x1, Pallas kernels, shards(): pl.pallas_call(kernel, out_shape=(jax.ShapeDtypeStruct((2, 8, 128, 128),...  37.3 us
    pallas_call x1, Pallas kernels, shards(): pl.pallas_call(write_out, out_shape=tuple((jax.ShapeDtypeStruct(v.shape,...  0.84 us

profile of v4, /device:TPU:1, one launch (start us, length us, event | category | flops | bytes accessed | tf_op | source)
XLA Modules:
  0.0 38.8 jit_solution(8011262138581600587)
XLA Ops:
  0.6 37.3 %shard_map.120 = (bf16[2,8,128,128]{3,2,1,0:T(8,128)(2,1)S(1)}, f32[2,8,128]{2,1,0:T(8,128)S(1)}, f32[2,8]{1,0:T(2,128)S(1)}, bf16[8,128]{1,0:T(8,128)(2,1)S(1)}) custom-call(bf16[128,16,1024]{2,1,0:T(8,128)(2,1)} %prompt.1, bf16[1024,128]{1,0:T(8,128)(2,1)} %bitcast.17, bf16[1024,128]{1,0:T(8,128)(2,1)} %bitcast.18, bf16[2,1024]{1,0:T(2,128)(2,1)} %bitcast.20, ...), custom_call_target="tpu_custom_call" | custom-call | tf_op jit(solution)/shard_map/pallas_call | solution.py:313
  38.0 0.8 %shard_map.121 = (bf16[2,8,128,128]{3,2,1,0:T(8,128)(2,1)}, f32[2,8,128]{2,1,0:T(8,128)}, f32[2,8]{1,0:T(2,128)}, bf16[8,128]{1,0:T(8,128)(2,1)}) custom-call(bf16[2,8,128,128]{3,2,1,0:T(8,128)(2,1)S(1)} %get-tuple-element.12.memory, f32[2,8,128]{2,1,0:T(8,128)S(1)} %get-tuple-element.13.normal, f32[2,8]{1,0:T(2,128)S(1)} %get-tuple-element.14.stable, ...), custom_call_target="tpu_custom_call" | custom-call | tf_op jit(solution)/shard_map/pallas_call | solution.py:360

commit v5 on v4

--- a/solution.py
+++ b/solution.py
@@ -12,19 +12,20 @@
 TP = ("x", "c")
 F32 = jnp.float32
 BF16 = jnp.bfloat16
-FAR = 12
-
-
-OFFSETS = [(1, 0), (2, 0), (3, 0), (1, 1), (2, 1), (3, 1), (1, 3), (2, 3), (3, 3), (1, 2), (2, 2), (3, 2)]
-DIRECT = FAR - 12
+FAR = 8
+
+
+OFFSETS = [(2, 0), (2, 1), (3, 1), (1, 3), (2, 3), (1, 2), (2, 2), (3, 2)]
+MADE = [(1, 0), (3, 0), (1, 1), (3, 3)]
+DIRECT = FAR - 8
 NEAR = (1, 3, 2)
 
 
 def kernel(
     prompt, w_key, w_value, w_in, w_forget, in_bias, forget_bias, query, w_out,
     memory_out, normal_out, stable_out, read_out,
-    rows, weights, gate_rows, gate_w, biases, queries, query_w, out_w, keys, values, gates, scores, terms, parts,
-    load_sem, far_send, far_recv, line_in, near_send, near_recv, x_send, x_recv, swap_send, swap_recv, term_send, term_recv,
+    rows, weights, gate_rows, gate_w, biases, queries, query_w, out_w, keys, values, gates, scores, made_rows, made_keys, made_values, made_gates, terms, parts,
+    load_sem, far_send, far_recv, line_in, made_send, made_recv, near_send, near_recv, x_send, x_recv, swap_send, swap_recv, term_send, term_recv,
 ):
     z, y, x, c = (lax.axis_index(a) for a in ("z", "y", "x", "c"))
     here = z * 4 + y
@@ -47,6 +48,9 @@
         pltpu.make_async_copy(query, queries, load_sem.at[7]),
         pltpu.make_async_copy(w_out, out_w, load_sem.at[8]),
     ]
+    for q, (dz, dy) in enumerate(MADE):
+        there = (zs[dz] * 4 + ys[dy]) * 8
+        loads.append(pltpu.make_async_copy(prompt.at[pl.ds(there, 8)], made_rows.at[q], load_sem.at[9 + q]))
     for load in loads:
         load.start()
 
@@ -116,7 +120,7 @@
 
     for k in range(3, 0, -1):
         pl.semaphore_signal(line_in, inc=1, device_id={"y": ys[k]}, device_id_type=MESH)
-    for k in range(3):
+    for k in range(1):
         far(k).start()
 
     for load in loads:
@@ -142,21 +146,63 @@
     which_seq = lax.broadcasted_iota(jnp.int32, (8, 16, 128), 0)
     own_lane = lax.rem(lane, 8) == which_seq
 
+    def products(block):
+        both = jnp.dot(block, weights[...], preferred_element_type=F32)
+        pre = jnp.dot(block, gate_w[...], preferred_element_type=F32).reshape(8, 16, 128)
+        return both, jnp.sum(jnp.where(own_lane, pre, 0.0), axis=0)
+
+    def positions(src):
+        return pl.ds(pl.multiple_of(src * 16, 16), 16)
+
+    def score(src, key_rows):
+        every = jnp.dot(key_rows, query_w[...], preferred_element_type=F32).reshape(8, 16, 128)
+        scores[positions(src), :] = jnp.sum(jnp.where(own_lane, every, 0.0), axis=0)
+
     def project(src):
-        block = rows[src].reshape(128, 1024)
-        both = jnp.dot(block, weights[...], preferred_element_type=F32)
-        at = pl.ds(pl.multiple_of(src * 16, 16), 16)
+        both, pre = products(rows[src].reshape(128, 1024))
+        at = positions(src)
         key_rows = both[:, :128].astype(BF16)
         keys[:, at, :] = key_rows.reshape(8, 16, 128)
         values[:, at, :] = both[:, 128:].astype(BF16).reshape(8, 16, 128)
-        pre = jnp.dot(block, gate_w[...], preferred_element_type=F32).reshape(8, 16, 128)
-        gates[at, :] = jnp.sum(jnp.where(own_lane, pre, 0.0), axis=0)
-        score = jnp.dot(key_rows, query_w[...], preferred_element_type=F32).reshape(8, 16, 128)
-        scores[at, :] = jnp.sum(jnp.where(own_lane, score, 0.0), axis=0)
+        gates[at, :] = pre
+        score(src, key_rows)
+
+    def made(q, which):
+        dz, dy = MADE[q]
+        at = positions(here)
+        src, dst = (
+            (made_keys.at[q], keys.at[:, at, :]),
+            (made_values.at[q], values.at[:, at, :]),
+            (made_gates.at[q], gates.at[at, :]),
+        )[which]
+        return pltpu.make_async_remote_copy(
+            src_ref=src,
+            dst_ref=dst,
+            send_sem=made_send.at[q, which],
+            recv_sem=made_recv.at[q, which],
+            device_id={"z": zs[dz], "y": ys[dy]},
+            device_id_type=MESH,
+        )
+
+    def make(q):
+        both, pre = products(made_rows[q].reshape(128, 1024))
+        made_keys[q] = both[:, :128].astype(BF16).reshape(8, 16, 128)
+        made_values[q] = both[:, 128:].astype(BF16).reshape(8, 16, 128)
+        made_gates[q] = pre
+
+    def send_made(q):
+        for which in range(3):
+            made(q, which).start()
+
+    def finish_made(q):
+        for which in range(3):
+            made(q, which).wait_recv()
+        src = zs[-MADE[q][0]] * 4 + ys[-MADE[q][1]]
+        score(src, keys[:, positions(src), :].reshape(128, 128))
 
     project(here)
     pl.semaphore_wait(line_in, 3)
-    for k in range(3, 4):
+    for k in range(1, 5):
         far(k).start()
 
     def arrive(k):
@@ -165,8 +211,8 @@
         along_x(k, 1).start()
         if k >= DIRECT:
             along_x(k, 2).start()
-        if k + 4 < FAR:
-            far(k + 4).start()
+        if k + 5 < FAR:
+            far(k + 5).start()
 
     def relay(k):
         along_x(k, 0).wait_recv()
@@ -202,10 +248,14 @@
         events.append((k + 8, 3, start_swap, k))
         events.append((k + 10, 4, finish, k))
     for k in range(3):
-        if (2, 2, 4)[k]:
-            events.append(((2, 2, 4)[k], 5, start_near, k))
-        events.append(((6, 8, 10)[k], 6, swap_near, k))
-        events.append(((9, 11, 13)[k], 7, finish_near, k))
+        if (1, 1, 3)[k]:
+            events.append(((1, 1, 3)[k], 5, start_near, k))
+        events.append(((6, 7, 8)[k], 6, swap_near, k))
+        events.append(((9, 10, 11)[k], 7, finish_near, k))
+    for q in range(len(MADE)):
+        events.append(((-1, 0, 1, 2)[q], 7, make, q))
+        events.append(((5, 5, 6, 7)[q], 8, send_made, q))
+        events.append(((12, 13, 14, 15)[q], 9, finish_made, q))
     for _, _, stage, k in sorted(events, key=lambda e: (e[0], e[1], e[3])):
         stage(k)
 
@@ -281,6 +331,9 @@
         for which in range(3):
             along_x(k, which).wait_send()
 
+    for q in range(len(MADE)):
+        for which in range(3):
+            made(q, which).wait_send()
     for k in range(3):
         near(k).wait_send()
         swap(FAR + k, near_source(k)).wait_send()
@@ -333,12 +386,18 @@
             pltpu.VMEM((8, 256, 128), BF16),
             pltpu.VMEM((256, 128), F32),
             pltpu.VMEM((256, 128), F32),
+            pltpu.VMEM((4, 8, 16, 1024), BF16),
+            pltpu.VMEM((4, 8, 16, 128), BF16),
+            pltpu.VMEM((4, 8, 16, 128), BF16),
+            pltpu.VMEM((4, 16, 128), F32),
             pltpu.VMEM((8, 8, 128), F32),
             pltpu.VMEM((8, 8, 128), F32),
-            dma((9,)),
+            dma((13,)),
             dma((FAR,)),
             dma((FAR,)),
             pltpu.SemaphoreType.REGULAR,
+            dma((4, 3)),
+            dma((4, 3)),
             dma((3,)),
             dma((3,)),
             dma((FAR, 3)),

time: 38.9 us -> 36.5 us (0.938)
  Pallas kernels: 38.2 us -> 35.8 us
    pallas_call x1, Pallas kernels: 37.3 us -> 34.9 us  [shards(): pl.pallas_call(kernel, out_shape=(jax.ShapeDtypeStruct((2, 8, 128, 128),...]
where the time goes in v5:
time: 36.5 us; the launch traced here: 36.4 us
  Pallas kernels  35.8 us (98%)
  between operations  0.64 us (2%)
    pallas_call x1, Pallas kernels, shards(): pl.pallas_call(kernel, out_shape=(jax.ShapeDtypeStruct((2, 8, 128, 128),...  34.9 us
    pallas_call x1, Pallas kernels, shards(): pl.pallas_call(write_out, out_shape=tuple((jax.ShapeDtypeStruct(v.shape,...  0.84 us

profile of v5, /device:TPU:1, one launch (start us, length us, event | category | flops | bytes accessed | tf_op | source)
XLA Modules:
  0.0 36.4 jit_solution(9975076503231718410)
XLA Ops:
  0.6 34.9 %shard_map.120 = (bf16[2,8,128,128]{3,2,1,0:T(8,128)(2,1)S(1)}, f32[2,8,128]{2,1,0:T(8,128)S(1)}, f32[2,8]{1,0:T(2,128)S(1)}, bf16[8,128]{1,0:T(8,128)(2,1)S(1)}) custom-call(bf16[128,16,1024]{2,1,0:T(8,128)(2,1)} %prompt.1, bf16[1024,128]{1,0:T(8,128)(2,1)} %bitcast.17, bf16[1024,128]{1,0:T(8,128)(2,1)} %bitcast.18, bf16[2,1024]{1,0:T(2,128)(2,1)} %bitcast.20, ...), custom_call_target="tpu_custom_call" | custom-call | tf_op jit(solution)/shard_map/pallas_call | solution.py:366
  35.6 0.8 %shard_map.121 = (bf16[2,8,128,128]{3,2,1,0:T(8,128)(2,1)}, f32[2,8,128]{2,1,0:T(8,128)}, f32[2,8]{1,0:T(2,128)}, bf16[8,128]{1,0:T(8,128)(2,1)}) custom-call(bf16[2,8,128,128]{3,2,1,0:T(8,128)(2,1)S(1)} %get-tuple-element.12.memory, f32[2,8,128]{2,1,0:T(8,128)S(1)} %get-tuple-element.13.normal, f32[2,8]{1,0:T(2,128)S(1)} %get-tuple-element.14.stable, ...), custom_call_target="tpu_custom_call" | custom-call | tf_op jit(solution)/shard_map/pallas_call | solution.py:419

commit v6 on v5

--- a/solution.py
+++ b/solution.py
@@ -122,6 +122,9 @@
         pl.semaphore_signal(line_in, inc=1, device_id={"y": ys[k]}, device_id_type=MESH)
     for k in range(1):
         far(k).start()
+    near(0).start()
+    near(1).start()
+    near(2).start()
 
     for load in loads:
         load.wait()
@@ -245,11 +248,11 @@
         events.append((k, 0, arrive, k))
         if k < DIRECT:
             events.append((k + 3, 2, relay, k))
-        events.append((k + 8, 3, start_swap, k))
-        events.append((k + 10, 4, finish, k))
+        events.append((k + 7, 3, start_swap, k))
+        events.append((k + 9, 4, finish, k))
     for k in range(3):
-        if (1, 1, 3)[k]:
-            events.append(((1, 1, 3)[k], 5, start_near, k))
+        if (0, 0, 0)[k]:
+            events.append(((0, 0, 0)[k], 5, start_near, k))
         events.append(((6, 7, 8)[k], 6, swap_near, k))
         events.append(((9, 10, 11)[k], 7, finish_near, k))
     for q in range(len(MADE)):

time: 36.5 us -> 35.8 us (0.981)
  Pallas kernels: 35.8 us -> 35.1 us
    pallas_call x1, Pallas kernels: 34.9 us -> 34.2 us  [shards(): pl.pallas_call(kernel, out_shape=(jax.ShapeDtypeStruct((2, 8, 128, 128),...]
where the time goes in v6:
time: 35.8 us; the launch traced here: 35.7 us
  Pallas kernels  35.1 us (98%)
  between operations  0.64 us (2%)
    pallas_call x1, Pallas kernels, shards(): pl.pallas_call(kernel, out_shape=(jax.ShapeDtypeStruct((2, 8, 128, 128),...  34.2 us
    pallas_call x1, Pallas kernels, shards(): pl.pallas_call(write_out, out_shape=tuple((jax.ShapeDtypeStruct(v.shape,...  0.84 us

profile of v6, /device:TPU:1, one launch (start us, length us, event | category | flops | bytes accessed | tf_op | source)
XLA Modules:
  0.0 35.7 jit_solution(13690583948671181147)
XLA Ops:
  0.6 34.2 %shard_map.120 = (bf16[2,8,128,128]{3,2,1,0:T(8,128)(2,1)S(1)}, f32[2,8,128]{2,1,0:T(8,128)S(1)}, f32[2,8]{1,0:T(2,128)S(1)}, bf16[8,128]{1,0:T(8,128)(2,1)S(1)}) custom-call(bf16[128,16,1024]{2,1,0:T(8,128)(2,1)} %prompt.1, bf16[1024,128]{1,0:T(8,128)(2,1)} %bitcast.17, bf16[1024,128]{1,0:T(8,128)(2,1)} %bitcast.18, bf16[2,1024]{1,0:T(2,128)(2,1)} %bitcast.20, ...), custom_call_target="tpu_custom_call" | custom-call | tf_op jit(solution)/shard_map/pallas_call | solution.py:369
  34.9 0.8 %shard_map.121 = (bf16[2,8,128,128]{3,2,1,0:T(8,128)(2,1)}, f32[2,8,128]{2,1,0:T(8,128)}, f32[2,8]{1,0:T(2,128)}, bf16[8,128]{1,0:T(8,128)(2,1)}) custom-call(bf16[2,8,128,128]{3,2,1,0:T(8,128)(2,1)S(1)} %get-tuple-element.12.memory, f32[2,8,128]{2,1,0:T(8,128)S(1)} %get-tuple-element.13.normal, f32[2,8]{1,0:T(2,128)S(1)} %get-tuple-element.14.stable, ...), custom_call_target="tpu_custom_call" | custom-call | tf_op jit(solution)/shard_map/pallas_call | solution.py:422

commit v7 on v6

--- a/solution.py
+++ b/solution.py
@@ -253,8 +253,8 @@
     for k in range(3):
         if (0, 0, 0)[k]:
             events.append(((0, 0, 0)[k], 5, start_near, k))
-        events.append(((6, 7, 8)[k], 6, swap_near, k))
-        events.append(((9, 10, 11)[k], 7, finish_near, k))
+        events.append(((4, 5, 6)[k], 6, swap_near, k))
+        events.append(((6, 7, 8)[k], 7, finish_near, k))
     for q in range(len(MADE)):
         events.append(((-1, 0, 1, 2)[q], 7, make, q))
         events.append(((5, 5, 6, 7)[q], 8, send_made, q))
@@ -272,8 +272,15 @@
     forget = pltpu.roll(jax.nn.log_sigmoid(pre), 112, 1)
     row = lax.broadcasted_iota(jnp.int32, (256, 256), 0)
     col = lax.broadcasted_iota(jnp.int32, (256, 256), 1)
-    lower = jnp.where(col < row, 1.0, 0.0)
-    before = jnp.dot(lower, forget, preferred_element_type=F32, precision=lax.Precision.HIGHEST)
+    lower = jnp.where(col < row, 1.0, 0.0).astype(BF16)
+    high = forget.astype(BF16).astype(F32)
+    middle = (forget - high).astype(BF16).astype(F32)
+    low = forget - high - middle
+    split = jnp.where(
+        lane1 < 16, high, jnp.where(lane1 < 32, pltpu.roll(middle, 16, 1), jnp.where(lane1 < 48, pltpu.roll(low, 32, 1), 0.0))
+    )
+    sums = jnp.dot(lower, split.astype(BF16), preferred_element_type=F32)
+    before = sums + pltpu.roll(sums, 112, 1) + pltpu.roll(sums, 96, 1)
     total = before[255:256, :] + forget[255:256, :]
     log_weight = pre + jnp.where(lane1 < 8, total - before - forget, before)
     stable = jnp.maximum(total, jnp.max(log_weight, axis=0, keepdims=True))

time: 35.8 us -> 35.7 us (level)
  no operation moved by 1% of the time
where the time goes in v7:
time: 35.7 us; the launch traced here: 35.6 us
  Pallas kernels  35 us (98%)
  between operations  0.64 us (2%)
    pallas_call x1, Pallas kernels, shards(): pl.pallas_call(kernel, out_shape=(jax.ShapeDtypeStruct((2, 8, 128, 128),...  34.1 us
    pallas_call x1, Pallas kernels, shards(): pl.pallas_call(write_out, out_shape=tuple((jax.ShapeDtypeStruct(v.shape,...  0.84 us

profile of v7, /device:TPU:1, one launch (start us, length us, event | category | flops | bytes accessed | tf_op | source)
XLA Modules:
  0.0 35.6 jit_solution(3828291806214442606)
XLA Ops:
  0.6 34.1 %shard_map.120 = (bf16[2,8,128,128]{3,2,1,0:T(8,128)(2,1)S(1)}, f32[2,8,128]{2,1,0:T(8,128)S(1)}, f32[2,8]{1,0:T(2,128)S(1)}, bf16[8,128]{1,0:T(8,128)(2,1)S(1)}) custom-call(bf16[128,16,1024]{2,1,0:T(8,128)(2,1)} %prompt.1, bf16[1024,128]{1,0:T(8,128)(2,1)} %bitcast.17, bf16[1024,128]{1,0:T(8,128)(2,1)} %bitcast.18, bf16[2,1024]{1,0:T(2,128)(2,1)} %bitcast.20, ...), custom_call_target="tpu_custom_call" | custom-call | tf_op jit(solution)/shard_map/pallas_call | solution.py:376
  34.8 0.8 %shard_map.121 = (bf16[2,8,128,128]{3,2,1,0:T(8,128)(2,1)}, f32[2,8,128]{2,1,0:T(8,128)}, f32[2,8]{1,0:T(2,128)}, bf16[8,128]{1,0:T(8,128)(2,1)}) custom-call(bf16[2,8,128,128]{3,2,1,0:T(8,128)(2,1)S(1)} %get-tuple-element.12.memory, f32[2,8,128]{2,1,0:T(8,128)S(1)} %get-tuple-element.13.normal, f32[2,8]{1,0:T(2,128)S(1)} %get-tuple-element.14.stable, ...), custom_call_target="tpu_custom_call" | custom-call | tf_op jit(solution)/shard_map/pallas_call | solution.py:429

commit v8 on v7

--- a/solution.py
+++ b/solution.py
@@ -51,9 +51,6 @@
     for q, (dz, dy) in enumerate(MADE):
         there = (zs[dz] * 4 + ys[dy]) * 8
         loads.append(pltpu.make_async_copy(prompt.at[pl.ds(there, 8)], made_rows.at[q], load_sem.at[9 + q]))
-    for load in loads:
-        load.start()
-
     barrier = pltpu.get_barrier_semaphore()
 
     for k in range(3, 0, -1):
@@ -63,6 +60,8 @@
         to = {"x": xs[k // 2], "c": cs[k % 2]}
         pl.semaphore_signal(barrier, inc=1, device_id=to, device_id_type=MESH)
 
+    for load in loads:
+        load.start()
     pl.semaphore_wait(barrier, 13)
 
     def far(k):

time: 35.7 us -> 36.2 us (1.014)
  Pallas kernels: 35 us -> 35.5 us
    pallas_call x1, Pallas kernels: 34.1 us -> 34.6 us  [shards(): pl.pallas_call(kernel, out_shape=(jax.ShapeDtypeStruct((2, 8, 128, 128),...]
where the time goes in v8:
time: 36.2 us; the launch traced here: 36.1 us
  Pallas kernels  35.5 us (98%)
  between operations  0.64 us (2%)
    pallas_call x1, Pallas kernels, shards(): pl.pallas_call(kernel, out_shape=(jax.ShapeDtypeStruct((2, 8, 128, 128),...  34.6 us
    pallas_call x1, Pallas kernels, shards(): pl.pallas_call(write_out, out_shape=tuple((jax.ShapeDtypeStruct(v.shape,...  0.84 us

profile of v8, /device:TPU:1, one launch (start us, length us, event | category | flops | bytes accessed | tf_op | source)
XLA Modules:
  0.0 36.1 jit_solution(14277557600916495703)
XLA Ops:
  0.6 34.6 %shard_map.120 = (bf16[2,8,128,128]{3,2,1,0:T(8,128)(2,1)S(1)}, f32[2,8,128]{2,1,0:T(8,128)S(1)}, f32[2,8]{1,0:T(2,128)S(1)}, bf16[8,128]{1,0:T(8,128)(2,1)S(1)}) custom-call(bf16[128,16,1024]{2,1,0:T(8,128)(2,1)} %prompt.1, bf16[1024,128]{1,0:T(8,128)(2,1)} %bitcast.17, bf16[1024,128]{1,0:T(8,128)(2,1)} %bitcast.18, bf16[2,1024]{1,0:T(2,128)(2,1)} %bitcast.20, ...), custom_call_target="tpu_custom_call" | custom-call | tf_op jit(solution)/shard_map/pallas_call | solution.py:375
  35.3 0.8 %shard_map.121 = (bf16[2,8,128,128]{3,2,1,0:T(8,128)(2,1)}, f32[2,8,128]{2,1,0:T(8,128)}, f32[2,8]{1,0:T(2,128)}, bf16[8,128]{1,0:T(8,128)(2,1)}) custom-call(bf16[2,8,128,128]{3,2,1,0:T(8,128)(2,1)S(1)} %get-tuple-element.12.memory, f32[2,8,128]{2,1,0:T(8,128)S(1)} %get-tuple-element.13.normal, f32[2,8]{1,0:T(2,128)S(1)} %get-tuple-element.14.stable, ...), custom_call_target="tpu_custom_call" | custom-call | tf_op jit(solution)/shard_map/pallas_call | solution.py:428
